TPU v7x, 32 devices: a whole 2x2x4 slice. The times are simulated.
32 devices in a mesh: ep: 8 (over z, core), tp: 4 (over y, x).
Axes of the slice: x: 2, y: 2, z: 4, core: 2. Of those that a mesh axis runs over, the one named last changes fastest.
Arguments:
- tokens: bfloat16 [128, 2048], P('ep'), may hold values from -6 to 6
- norm_gain: float32 [2048], replicated, may hold values from 0.1 to 1.9
- w_query: bfloat16 [2048, 512], P('ep', 'tp'), may hold values from -0.125 to 0.125
- w_key: bfloat16 [2048, 512], P('ep', 'tp'), may hold values from -0.125 to 0.125
- w_decay: bfloat16 [2048, 512], P('ep', 'tp'), may hold values from -0.125 to 0.125
- w_value: bfloat16 [2048, 1024], P('ep', 'tp'), may hold values from -0.125 to 0.125
- w_outgate: bfloat16 [2048, 1024], P('ep', 'tp'), may hold values from -0.125 to 0.125
- decay_rate: float32 [512], P('tp'), may hold values from 0.02 to 1
- state: float32 [128, 4, 128, 256], P('ep', 'tp'), may hold values from -15 to 15
- head_gain: float32 [256], replicated, may hold values from 0.1 to 1.9
- w_output: bfloat16 [1024, 2048], P('tp'), may hold values from -0.1875 to 0.1875
- moe_gain: float32 [2048], replicated, may hold values from 0.1 to 1.9
- expert_ids: int32 [128, 2], P('ep'), may hold values from 0 to 7, all different within a row; in each aligned block of 16 rows (0 to 15, 16 to 31, ...) at most 8 rows name the same one
- group_prob: float32 [128], P('ep'), may hold values from 0.3 to 1
- inner_prob: float32 [128, 2], P('ep'), may hold values from 0.05 to 1
- w_gate: bfloat16 [8, 2048, 2048], P('ep', None, 'tp'), may hold values from -0.125 to 0.125
- w_up: bfloat16 [8, 2048, 2048], P('ep', None, 'tp'), may hold values from -0.125 to 0.125
- w_down: bfloat16 [8, 2048, 2048], P('ep', 'tp'), may hold values from -0.125 to 0.125
Outputs:
- output: bfloat16 [128, 2048], P('ep', 'tp')
Inputs may be any that keep to these rules, and one draw needn't show every extreme that they name: `expert_ids`: the 2 experts of a token differ. In the rows of one index of ep no expert is named more than 8 times, a bound that some block reaches there.
All inputs are finite; a program needn't handle non-finite values.
Results may differ from a plain program's by a relative error of at most 0.025.
Values may be sent and summed in bfloat16 or wider, within the bound.
No kernel may reach another device: no remote copies, remote signals or barrier semaphores. Data moves between devices by JAX's collectives and lax.ppermute only.
A program may use at most 64 MiB of HBM per device.

v0:
```python
import functools

import jax
import jax.numpy as jnp
from jax import lax
from jax.experimental import pallas as pl
from jax.experimental.pallas import tpu as pltpu
from jax.sharding import PartitionSpec as P


epsilon = 1e-05
wide = jnp.float32
narrow = jnp.bfloat16
lane_tile = 128


def inverse_rms(values):
    return lax.rsqrt(jnp.mean(values * values, axis=-1, keepdims=True) + epsilon)


def silu(values):
    return values / (1.0 + jnp.exp(-values))


def swap_core(block):
    count = lax.axis_size("ep")
    return lax.ppermute(block, "ep", [(i, i ^ 1) for i in range(count)])


def swap_chips(blocks):
    count = lax.axis_size("ep")
    got = {}
    for k in range(len(blocks) - 1, 0, -1):
        got[k] = lax.ppermute(blocks[k], "ep", [(i, i ^ (2 * k + 1)) for i in range(count)])
    return [got[k] for k in range(1, len(blocks))]


def swap_heads(blocks, other_core):
    ep_count, count = lax.axis_size("ep"), lax.axis_size("tp")
    got = {}
    for k in range(len(blocks) - 1, 0, -1):
        pairs = [
            (e * count + t, (e ^ other_core) * count + (t ^ k))
            for e in range(ep_count)
            for t in range(count)
        ]
        got[k] = lax.ppermute(blocks[k], ("ep", "tp"), pairs)
    return [got[k] for k in range(1, len(blocks))]


def call(kernel, outs, args, limit, flops=0):
    nbytes = sum(a.size * a.dtype.itemsize for a in args)
    nbytes += sum(o.size * o.dtype.itemsize for o in outs)
    return pl.pallas_call(
        kernel,
        out_shape=tuple(outs),
        in_specs=[pl.BlockSpec(memory_space=pltpu.VMEM)] * len(args),
        out_specs=tuple(pl.BlockSpec(memory_space=pltpu.VMEM) for _ in outs),
        compiler_params=pltpu.CompilerParams(vmem_limit_bytes=limit),
        cost_estimate=pl.CostEstimate(flops=flops, bytes_accessed=nbytes, transcendentals=0),
    )(*args)


def load_call(kernel, args, extra):
    outs = [like(a.shape, a.dtype) for a in args] + list(extra)
    return pl.pallas_call(
        functools.partial(kernel, len(args)),
        out_shape=tuple(outs),
        in_specs=[pl.BlockSpec(memory_space=pltpu.HBM)] * len(args),
        out_specs=tuple(pl.BlockSpec(memory_space=pltpu.VMEM) for _ in outs),
        scratch_shapes=[pltpu.SemaphoreType.DMA((len(args),))],
        compiler_params=pltpu.CompilerParams(vmem_limit_bytes=2 << 20),
        cost_estimate=pl.CostEstimate(flops=1 << 22, bytes_accessed=1 << 22, transcendentals=0),
    )(*[pltpu.with_memory_space_constraint(a, pltpu.HBM) for a in args])


def like(shape, dtype):
    return jax.ShapeDtypeStruct(shape, dtype)


def spread_kernel(tokens_ref, *out_refs):
    chip = lax.axis_index("ep") // 2
    cols = out_refs[0].shape[1]
    for k, out in enumerate(out_refs):
        out[...] = tokens_ref[:, pl.ds(pl.multiple_of((chip ^ k) * cols, lane_tile), cols)]


def load(pairs, sems):
    copies = [pltpu.make_async_copy(src, dst, sems.at[n]) for n, (src, dst) in enumerate(pairs)]
    for copy in copies:
        copy.start()
    return copies


def load_kernel(count, *refs):
    for copy in load(list(zip(refs[:count], refs[count : 2 * count])), refs[-1]):
        copy.wait()


def side_kernel(count, *refs):
    loaded = refs[count : 2 * count]
    scale_ref, share_ref, sems = refs[2 * count :]
    copies = load(list(zip(refs[:count], loaded)), sems)
    for copy in copies[:4]:
        copy.wait()
    tokens_ref, ids_ref, group_ref, inner_ref = loaded[:4]
    experts = lax.axis_size("ep")
    scale_ref[...] = jnp.broadcast_to(inverse_rms(tokens_ref[...].astype(wide)), scale_ref.shape)
    lanes, seqs = share_ref.shape[1], share_ref.shape[0]
    inner = inner_ref[...]
    weight = group_ref[...] * inner / jnp.sum(inner, axis=0, keepdims=True)
    place = lax.broadcasted_iota(jnp.int32, (lanes, seqs), 0)
    owner = jnp.where(place >= experts, place - experts, place)
    share = jnp.zeros((lanes, seqs), wide)
    for k in range(ids_ref.shape[0]):
        share = share + jnp.where(owner == ids_ref[k : k + 1, :], weight[k : k + 1, :], 0.0)
    high = share.astype(narrow).astype(wide)
    packed = jnp.where(place < experts, high, jnp.where(place < 2 * experts, share - high, 0.0))
    share_ref[...] = packed.T.astype(narrow)
    for copy in copies[4:]:
        copy.wait()


def project_kernel(chips, gain_ref, *refs):
    blocks, refs = refs[: 2 * chips], refs[2 * chips :]
    weights, (own_ref, away_ref) = refs[:-2], refs[-2:]
    me = lax.axis_index("ep")
    south = me % 2 == 0
    feats = weights[0].shape[0]
    pair_gain = gain_ref[:, pl.ds(pl.multiple_of(me // 2 * 2 * feats, lane_tile), 2 * feats)]
    rows = jnp.concatenate([block[...] for block in blocks], axis=0).astype(wide) * pair_gain
    rows = jnp.where(south, rows[:, :feats], rows[:, feats:]).astype(narrow)
    half = own_ref.shape[0]
    at = 0
    for weight in weights:
        cols = weight.shape[1]
        product = jnp.dot(rows, weight[...], preferred_element_type=wide)
        own_ref[:, at : at + cols] = product[:half]
        away_ref[:, at : at + cols] = product[half:].astype(narrow)
        at += cols


def recurrent_kernel(chips, cuts, base_ref, *refs):
    arrived, refs = refs[: chips - 1], refs[chips - 1 :]
    scale_ref, rate_ref, state_ref, gain_ref, output_ref, part_ref, read_ref = refs
    query_cols, value_cols = cuts
    seqs, heads, key_width, value_width = state_ref.shape
    total = base_ref[...]
    for block in arrived:
        total = total + block[...].astype(wide)
    total = total * scale_ref[:, :1]
    rounded = total.astype(narrow).astype(wide)
    pre = total[:, 2 * query_cols : 3 * query_cols]
    log_gate = jnp.minimum(pre, 0.0) - jnp.log1p(jnp.exp(-jnp.abs(pre)))
    decay = jnp.exp(log_gate * rate_ref[...])
    query = rounded[:, :query_cols] * key_width ** (-0.5)
    keys = rounded[:, query_cols : 2 * query_cols]
    turned = (query * decay).T
    out = None
    for h in range(heads):
        span = slice(h * key_width, (h + 1) * key_width)
        at = 3 * query_cols + h * value_width
        values = rounded[:, at : at + value_width]
        gates = rounded[:, at + value_cols : at + value_cols + value_width]
        for s in range(seqs):
            column = turned[span, s : s + 1]
            read_ref[s : s + 1, :] = jnp.sum(column * state_ref[s, h], axis=0, keepdims=True)
        match = jnp.sum(query[:, span] * keys[:, span], axis=1, keepdims=True)
        readout = read_ref[...] + match * values
        gated = (readout * inverse_rms(readout) * gain_ref[...] * silu(gates)).astype(narrow)
        rows = slice(h * value_width, (h + 1) * value_width)
        part = jnp.dot(gated, output_ref[rows, :], preferred_element_type=wide)
        out = part if out is None else out + part
    part_ref[...] = out.astype(narrow)


def mix_kernel(others, tokens_ref, part_ref, *refs):
    arrived, (gain_ref, share_ref, send_ref, own_ref) = refs[:others], refs[others:]
    width = tokens_ref.shape[1]
    attention = part_ref[...].astype(wide)
    for block in arrived:
        attention = attention + block[...].astype(wide)
    mixed = (tokens_ref[...].astype(wide) + attention).astype(narrow).astype(wide)
    send_ref[:, :width] = (mixed * inverse_rms(mixed) * gain_ref[...]).astype(narrow)
    send_ref[:, width:] = share_ref[...]
    cols = own_ref.shape[1]
    head = lax.axis_index("tp")
    attention = jnp.zeros(own_ref.shape, wide)
    at = pl.ds(pl.multiple_of(head * cols, lane_tile), cols)
    for block in (part_ref, *arrived):
        attention = attention + block[:, at].astype(wide)
    own_ref[...] = (tokens_ref[:, at].astype(wide) + attention).astype(narrow).astype(wide)


def expert_kernel(count, *refs):
    blocks, (gate_ref, up_ref, down_ref, own_ref, away_ref) = refs[:count], refs[count:]
    width = gate_ref.shape[1]
    rows = jnp.concatenate([block[:, :width] for block in blocks], axis=0)
    share = jnp.concatenate([block[:, width:] for block in blocks], axis=0).astype(wide)
    me, experts = lax.axis_index("ep"), lax.axis_size("ep")
    place = lax.broadcasted_iota(jnp.int32, share.shape, 1)
    chosen = (place == me) | (place == me + experts)
    weight = jnp.sum(jnp.where(chosen, share, 0.0), axis=1, keepdims=True)
    gate = jnp.dot(rows, gate_ref[0], preferred_element_type=wide)
    upper = jnp.dot(rows, up_ref[0], preferred_element_type=wide)
    hidden = (silu(gate) * upper).astype(narrow)
    head = lax.axis_index("tp")
    pieces, half, cols = own_ref.shape
    for k in range(pieces):
        at = pl.ds(pl.multiple_of((head ^ k) * cols, lane_tile), cols)
        out = jnp.dot(hidden, down_ref[0, :, at], preferred_element_type=wide) * weight
        near, far = (out[:half], out[half:]) if k == 0 else (out[half:], out[:half])
        own_ref[k] = near
        away_ref[k] = far.astype(narrow)


def on_device(
    tokens,
    norm_gain,
    w_query,
    w_key,
    w_decay,
    w_value,
    w_outgate,
    decay_rate,
    state,
    head_gain,
    w_output,
    moe_gain,
    expert_ids,
    group_prob,
    inner_prob,
    w_gate,
    w_up,
    w_down,
):
    seqs, width = tokens.shape
    ep_count, tp_count = lax.axis_size("ep"), lax.axis_size("tp")
    chips = ep_count // 2
    half = chips * seqs
    _, _, value_width = state.shape[1:]
    feats = w_query.shape[0]
    query_cols, value_cols = w_query.shape[1], w_value.shape[1]
    proj_cols = 3 * query_cols + 2 * value_cols
    cols = width // tp_count
    lanes = -(-2 * ep_count // lane_tile) * lane_tile
    mib = 1 << 20

    pair_cols = call(spread_kernel, [like((seqs, 2 * feats), narrow)] * chips, (tokens,), 4 * mib)
    blocks = [pair_cols[0], *swap_chips(pair_cols)]
    blocks += [swap_core(block) for block in blocks]
    side_args = (
        tokens,
        expert_ids.T,
        group_prob[None, :],
        inner_prob.T,
        norm_gain[None, :],
        w_query,
        w_key,
        w_decay,
        w_value,
        w_outgate,
        decay_rate[None, :],
        head_gain[None, :],
        moe_gain[None, :],
        w_output,
        state,
    )
    loaded = load_call(
        side_kernel, side_args, [like((seqs, lane_tile), wide), like((seqs, lanes), narrow)]
    )
    tokens_near = loaded[0]
    gain, weights = loaded[4], loaded[5:10]
    rate, read_gain, mix_gain, output_near, state_near, scale, share = loaded[10:]
    own, away = call(
        functools.partial(project_kernel, chips),
        [like((half, proj_cols), wide), like((half, proj_cols), narrow)],
        (gain, *blocks, *weights),
        8 * mib,
    )
    both = own + swap_core(away).astype(wide)
    both_narrow = both.astype(narrow)
    arrived = swap_chips([both_narrow[k * seqs : (k + 1) * seqs] for k in range(chips)])
    expert_weights = load_call(load_kernel, (w_gate, w_up, w_down), [])
    (part,) = pl.pallas_call(
        functools.partial(recurrent_kernel, chips, (query_cols, value_cols)),
        out_shape=(like((seqs, width), narrow),),
        in_specs=[pl.BlockSpec(memory_space=pltpu.VMEM)] * (chips + 5),
        out_specs=(pl.BlockSpec(memory_space=pltpu.VMEM),),
        scratch_shapes=[pltpu.VMEM((seqs, value_width), wide)],
        compiler_params=pltpu.CompilerParams(vmem_limit_bytes=8 * mib),
        cost_estimate=pl.CostEstimate(flops=1 << 20, bytes_accessed=4 << 20, transcendentals=0),
        name="recurrent",
    )(both[:seqs], *arrived, scale, rate, state_near, read_gain, output_near)
    parts = swap_heads([part] * tp_count, 0)
    sending, mixed_own = call(
        functools.partial(mix_kernel, tp_count - 1),
        [like((seqs, width + lanes), narrow), like((seqs, cols), wide)],
        (tokens_near, part, *parts, mix_gain, share),
        4 * mib,
    )
    rows = [sending, *swap_chips([sending] * chips)]
    rows += [swap_core(block) for block in rows]
    own, away = call(
        functools.partial(expert_kernel, 2 * chips),
        [like((tp_count, half, cols), wide), like((tp_count, half, cols), narrow)],
        (*rows, *expert_weights),
        24 * mib,
    )
    pair_sum = own + swap_core(away).astype(wide)
    pair_narrow = pair_sum.astype(narrow)
    head_sum = pair_sum[0]
    for block in swap_heads([pair_narrow[k] for k in range(tp_count)], 1):
        head_sum = head_sum + block.astype(wide)
    head_narrow = head_sum.astype(narrow)
    moe_sum = head_sum[:seqs]
    for block in swap_chips([head_narrow[k * seqs : (k + 1) * seqs] for k in range(chips)]):
        moe_sum = moe_sum + block.astype(wide)
    return (mixed_own + moe_sum).astype(narrow)


def solution(mesh):
    placed = (
        P("ep", None),
        P(),
        P("ep", "tp"),
        P("ep", "tp"),
        P("ep", "tp"),
        P("ep", "tp"),
        P("ep", "tp"),
        P("tp"),
        P("ep", "tp", None, None),
        P(),
        P("tp", None),
        P(),
        P("ep", None),
        P("ep"),
        P("ep", None),
        P("ep", None, "tp"),
        P("ep", None, "tp"),
        P("ep", "tp", None),
    )

    return jax.shard_map(
        on_device, mesh=mesh, in_specs=placed, out_specs=P("ep", "tp"), check_vma=False
    )
```

profile of v0, /device:TPU:0, one launch (start us, length us, event | category | flops | bytes accessed | tf_op | source)
XLA Modules:
  0.0 61.2 jit_solution(16070449414189378568)
XLA Ops:
  0.0 0.8 %copy-done = bf16[16,2048]{1,0:T(8,128)(2,1)S(1)} copy-done((bf16[16,2048]{1,0:T(8,128)(2,1)S(1)}, bf16[16,2048]{1,0:T(8,128)(2,1)}, u32[]{:S(2)}) %copy-start) | copy-done | bytes 65560
  0.8 2.5 %collective-permute-start = (bf16[16,512]{1,0:T(8,128)(2,1)S(1)}, bf16[16,512]{1,0:T(8,128)(2,1)S(1)}, u32[]{:S(2)}, u32[]{:S(2)}) collective-permute-start(bf16[16,512]{1,0:T(8,128)(2,1)S(1)} %get-tuple-element.35), channel_id=1, source_target_pairs={{0,12},{4,8},{8,4},{12,0},{16,28},{20,24},{24,20},{28,16},{1,13},{... | collective-permute-start | bytes 49160 | tf_op jit(solution)/shard_map/ppermute | solution.py:34
  3.3 2.9 %collective-permute-start.1 = (bf16[16,512]{1,0:T(8,128)(2,1)S(1)}, bf16[16,512]{1,0:T(8,128)(2,1)S(1)}, u32[]{:S(2)}, u32[]{:S(2)}) collective-permute-start(bf16[16,512]{1,0:T(8,128)(2,1)S(1)} %get-tuple-element.36), channel_id=1, source_target_pairs={{0,20},{4,16},{8,28},{12,24},{16,4},{20,0},{24,12},{28,8},{1,21},{... | collective-permute-start | bytes 49160 | tf_op jit(solution)/shard_map/ppermute | solution.py:34
  6.7 1.0 %collective-permute-done.1.refs_2_ = bf16[16,512]{1,0:T(8,128)(2,1)S(1)} collective-permute-done((bf16[16,512]{1,0:T(8,128)(2,1)S(1)}, bf16[16,512]{1,0:T(8,128)(2,1)S(1)}, u32[]{:S(2)}, u32[]{:S(2)}) %collective-permute-start.1) | collective-permute-done | bytes 16416 | tf_op jit(solution)/shard_map/ppermute | solution.py:34
  8.1 3.3 %collective-permute-done.2.refs_3_ = bf16[16,512]{1,0:T(8,128)(2,1)S(1)} collective-permute-done((bf16[16,512]{1,0:T(8,128)(2,1)S(1)}, bf16[16,512]{1,0:T(8,128)(2,1)S(1)}, u32[]{:S(2)}, u32[]{:S(2)}) %collective-permute-start.2) | collective-permute-done | bytes 16416 | tf_op jit(solution)/shard_map/ppermute | solution.py:34
  11.4 3.0 %shard_map.172 = (bf16[16,2048]{1,0:T(8,128)(2,1)S(1)}, s32[2,16]{1,0:T(2,128)}, f32[1,16]{1,0:T(1,128)}, f32[2,16]{1,0:T(2,128)}, f32[1,2048]{1,0:T(1,128)S(1)}...) custom-call(bf16[16,2048]{1,0:T(8,128)(2,1)} %tokens_ref.1, ...), custom_call_target="tpu_custom_call" | custom-call | flops 4194304 | bytes 4194304 | tf_op jit(solution)/shard_map/pallas_call | solution.py:66
  15.2 1.0 %collective-permute-done.7 = bf16[64,896]{1,0:T(8,128)(2,1)S(1)} collective-permute-done((bf16[64,896]{1,0:T(8,128)(2,1)S(1)}, bf16[64,896]{1,0:T(8,128)(2,1)S(1)}, u32[]{:S(2)}, u32[]{:S(2)}) %collective-permute-start.7) | collective-permute-done | bytes 114720 | tf_op jit(solution)/shard_map/ppermute | solution.py:27
  16.3 4.0 %collective-permute-start.8 = (bf16[16,896]{1,0:T(8,128)(2,1)S(1)}, bf16[16,896]{1,0:T(8,128)(2,1)S(1)}, u32[]{:S(2)}, u32[]{:S(2)}) collective-permute-start(bf16[16,896]{1,0:T(8,128)(2,1)S(1)} %get-tuple-element.70), channel_id=1, source_target_pairs={{0,12},{4,8},{8,4},{12,0},{16,28},{20,24},{24,20},{28,16},{1,13},{... | collective-permute-start | bytes 86024 | tf_op jit(solution)/shard_map/ppermute | solution.py:34
  20.3 1.0 %collective-permute-done.10.refs_2_ = bf16[16,896]{1,0:T(8,128)(2,1)S(1)} collective-permute-done((bf16[16,896]{1,0:T(8,128)(2,1)S(1)}, bf16[16,896]{1,0:T(8,128)(2,1)S(1)}, u32[]{:S(2)}, u32[]{:S(2)}) %collective-permute-start.10) | collective-permute-done | bytes 28704 | tf_op jit(solution)/shard_map/ppermute | solution.py:34
  21.4 0.9 %collective-permute-done.8.refs_0_ = bf16[16,896]{1,0:T(8,128)(2,1)S(1)} collective-permute-done((bf16[16,896]{1,0:T(8,128)(2,1)S(1)}, bf16[16,896]{1,0:T(8,128)(2,1)S(1)}, u32[]{:S(2)}, u32[]{:S(2)}) %collective-permute-start.8) | collective-permute-done | bytes 28704 | tf_op jit(solution)/shard_map/ppermute | solution.py:34
  22.3 1.0 %recurrent.1.part_ref = bf16[16,2048]{1,0:T(8,128)(2,1)S(1)} custom-call(f32[16,896]{1,0:T(8,128)S(1)} %slice.48.base_ref, bf16[16,896]{1,0:T(8,128)(2,1)S(1)} %collective-permute-done.8.refs_0_, bf16[16,896]{1,0:T(8,128)(2,1)S(1)} %collective-permute-done.9.refs_1_, bf16[16,896]{1,0:T(8,128)(2,1)S(1)} %collective-permute-done.10.refs_2_, ...), custom_call_target="tpu_custom_call" | custom-call | flops 1048576 | bytes 4194304 | tf_op jit(solution)/shard_map/recurrent/pallas_call | solution.py:285
  23.3 2.5 %collective-permute-start.13 = (bf16[16,2048]{1,0:T(8,128)(2,1)S(1)}, bf16[16,2048]{1,0:T(8,128)(2,1)S(1)}, u32[]{:S(2)}, u32[]{:S(2)}) collective-permute-start(bf16[16,2048]{1,0:T(8,128)(2,1)S(1)} %recurrent.1.part_ref), channel_id=1, source_target_pairs={{0,3},{1,2},{2,1},{3,0},{4,7},{5,6},{6,5},{7,4},{8,11},{9,10},{10,... | collective-permute-start | bytes 196616 | tf_op jit(solution)/shard_map/ppermute | solution.py:47
  26.2 0.5 collective-permute-start.11
  26.8 1.7 %collective-permute-done.13.refs_2_ = bf16[16,2048]{1,0:T(8,128)(2,1)S(1)} collective-permute-done((bf16[16,2048]{1,0:T(8,128)(2,1)S(1)}, bf16[16,2048]{1,0:T(8,128)(2,1)S(1)}, u32[]{:S(2)}, u32[]{:S(2)}) %collective-permute-start.13) | collective-permute-done | bytes 65568 | tf_op jit(solution)/shard_map/ppermute | solution.py:47
  28.5 1.5 %collective-permute-done.12.refs_1_ = bf16[16,2048]{1,0:T(8,128)(2,1)S(1)} collective-permute-done((bf16[16,2048]{1,0:T(8,128)(2,1)S(1)}, bf16[16,2048]{1,0:T(8,128)(2,1)S(1)}, u32[]{:S(2)}, u32[]{:S(2)}) %collective-permute-start.12) | collective-permute-done | bytes 65568 | tf_op jit(solution)/shard_map/ppermute | solution.py:47
  30.8 2.5 %collective-permute-start.15 = (bf16[16,2176]{1,0:T(8,128)(2,1)S(1)}, bf16[16,2176]{1,0:T(8,128)(2,1)S(1)}, u32[]{:S(2)}, u32[]{:S(2)}) collective-permute-start(bf16[16,2176]{1,0:T(8,128)(2,1)S(1)} %get-tuple-element.53.refs_0_), channel_id=1, source_target_pairs={{0,20},{4,16},{8,28},{12,24},{16,4},{20,0},{24,12},{28,8},{1,21},{... | collective-permute-start | bytes 208904 | tf_op jit(solution)/shard_map/ppermute | solution.py:34
  33.3 1.7 %collective-permute-start.17 = (bf16[16,2176]{1,0:T(8,128)(2,1)S(1)}, bf16[16,2176]{1,0:T(8,128)(2,1)S(1)}, u32[]{:S(2)}, u32[]{:S(2)}) collective-permute-start(bf16[16,2176]{1,0:T(8,128)(2,1)S(1)} %get-tuple-element.53.refs_0_), channel_id=1, source_target_pairs={{0,4},{4,0},{8,12},{12,8},{16,20},{20,16},{24,28},{28,24},{1,5},{5... | collective-permute-start | bytes 208904 | tf_op jit(solution)/shard_map/ppermute | solution.py:27
  35.0 2.0 %collective-permute-done.16.refs_3_ = bf16[16,2176]{1,0:T(8,128)(2,1)S(1)} collective-permute-done((bf16[16,2176]{1,0:T(8,128)(2,1)S(1)}, bf16[16,2176]{1,0:T(8,128)(2,1)S(1)}, u32[]{:S(2)}, u32[]{:S(2)}) %collective-permute-start.16) | collective-permute-done | bytes 69664 | tf_op jit(solution)/shard_map/ppermute | solution.py:34
  37.0 2.6 %collective-permute-done.15.refs_2_ = bf16[16,2176]{1,0:T(8,128)(2,1)S(1)} collective-permute-done((bf16[16,2176]{1,0:T(8,128)(2,1)S(1)}, bf16[16,2176]{1,0:T(8,128)(2,1)S(1)}, u32[]{:S(2)}, u32[]{:S(2)}) %collective-permute-start.15) | collective-permute-done | bytes 69664 | tf_op jit(solution)/shard_map/ppermute | solution.py:34
  40.1 2.9 %shard_map.176 = (bf16[1,2048,512]{2,1,0:T(8,128)(2,1)S(1)}, bf16[1,2048,512]{2,1,0:T(8,128)(2,1)S(1)}, bf16[1,512,2048]{2,1,0:T(8,128)(2,1)S(1)}) custom-call(bf16[1,2048,512]{2,1,0:T(8,128)(2,1)} %refs_0_.3, bf16[1,2048,512]{2,1,0:T(8,128)(2,1)} %refs_1_.1, bf16[1,512,2048]{2,1,0:T(8,128)(2,1)} %refs_2_.1), custom_call_target="tpu_custom_call" | custom-call | flops 4194304 | bytes 4194304 | tf_op jit(solution)/shard_map/pallas_call | solution.py:66
  43.1 1.1 %shard_map.177 = (f32[4,64,512]{2,1,0:T(8,128)S(1)}, bf16[4,64,512]{2,1,0:T(8,128)(2,1)S(1)}) custom-call(bf16[16,2176]{1,0:T(8,128)(2,1)S(1)} %get-tuple-element.53.refs_0_, bf16[16,2176]{1,0:T(8,128)(2,1)S(1)} %collective-permute-done.14.refs_1_, bf16[16,2176]{1,0:T(8,128)(2,1)S(1)} %collective-permute-done.15.refs_2_, ...), custom_call_target="tpu_custom_call" | custom-call | bytes 7634944 | tf_op jit(solution)/shard_map/pallas_call | solution.py:54
  44.3 1.5 %collective-permute-done.21 = bf16[4,64,512]{2,1,0:T(8,128)(2,1)S(1)} collective-permute-done((bf16[4,64,512]{2,1,0:T(8,128)(2,1)S(1)}, bf16[4,64,512]{2,1,0:T(8,128)(2,1)S(1)}, u32[]{:S(2)}, u32[]{:S(2)}) %collective-permute-start.21) | collective-permute-done | bytes 262176 | tf_op jit(solution)/shard_map/ppermute | solution.py:27
  45.9 1.5 %collective-permute-start.22 = (bf16[64,512]{1,0:T(8,128)(2,1)S(1)}, bf16[64,512]{1,0:T(8,128)(2,1)S(1)}, u32[]{:S(2)}, u32[]{:S(2)}) collective-permute-start(bf16[64,512]{1,0:T(8,128)(2,1)S(1)} %get-tuple-element.65), channel_id=1, source_target_pairs={{0,5},{1,4},{2,7},{3,6},{4,1},{5,0},{6,3},{7,2},{8,13},{9,12},{10,... | collective-permute-start | bytes 196616 | tf_op jit(solution)/shard_map/ppermute | solution.py:47
  47.4 1.8 %collective-permute-start.24 = (bf16[64,512]{1,0:T(8,128)(2,1)S(1)}, bf16[64,512]{1,0:T(8,128)(2,1)S(1)}, u32[]{:S(2)}, u32[]{:S(2)}) collective-permute-start(bf16[64,512]{1,0:T(8,128)(2,1)S(1)} %get-tuple-element.66), channel_id=1, source_target_pairs={{0,7},{1,6},{2,5},{3,4},{4,3},{5,2},{6,1},{7,0},{8,15},{9,14},{10,... | collective-permute-start | bytes 196616 | tf_op jit(solution)/shard_map/ppermute | solution.py:47
  49.2 0.8 %collective-permute-done.22 = bf16[64,512]{1,0:T(8,128)(2,1)S(1)} collective-permute-done((bf16[64,512]{1,0:T(8,128)(2,1)S(1)}, bf16[64,512]{1,0:T(8,128)(2,1)S(1)}, u32[]{:S(2)}, u32[]{:S(2)}) %collective-permute-start.22) | collective-permute-done | bytes 65568 | tf_op jit(solution)/shard_map/ppermute | solution.py:47
  50.0 3.0 %collective-permute-done.24 = bf16[64,512]{1,0:T(8,128)(2,1)S(1)} collective-permute-done((bf16[64,512]{1,0:T(8,128)(2,1)S(1)}, bf16[64,512]{1,0:T(8,128)(2,1)S(1)}, u32[]{:S(2)}, u32[]{:S(2)}) %collective-permute-start.24) | collective-permute-done | bytes 65568 | tf_op jit(solution)/shard_map/ppermute | solution.py:47
  53.0 1.6 %collective-permute-done.23 = bf16[64,512]{1,0:T(8,128)(2,1)S(1)} collective-permute-done((bf16[64,512]{1,0:T(8,128)(2,1)S(1)}, bf16[64,512]{1,0:T(8,128)(2,1)S(1)}, u32[]{:S(2)}, u32[]{:S(2)}) %collective-permute-start.23) | collective-permute-done | bytes 65568 | tf_op jit(solution)/shard_map/ppermute | solution.py:47
  54.8 0.9 %collective-permute-start.27 = (bf16[16,512]{1,0:T(8,128)(2,1)S(1)}, bf16[16,512]{1,0:T(8,128)(2,1)S(1)}, u32[]{:S(2)}, u32[]{:S(2)}) collective-permute-start(bf16[16,512]{1,0:T(8,128)(2,1)S(1)} %get-tuple-element.72), channel_id=1, source_target_pairs={{0,28},{4,24},{8,20},{12,16},{16,12},{20,8},{24,4},{28,0},{1,29},{... | collective-permute-start | bytes 49160 | tf_op jit(solution)/shard_map/ppermute | solution.py:34
  55.7 2.0 %collective-permute-start.26 = (bf16[16,512]{1,0:T(8,128)(2,1)S(1)}, bf16[16,512]{1,0:T(8,128)(2,1)S(1)}, u32[]{:S(2)}, u32[]{:S(2)}) collective-permute-start(bf16[16,512]{1,0:T(8,128)(2,1)S(1)} %get-tuple-element.73), channel_id=1, source_target_pairs={{0,20},{4,16},{8,28},{12,24},{16,4},{20,0},{24,12},{28,8},{1,21},{... | collective-permute-start | bytes 49160 | tf_op jit(solution)/shard_map/ppermute | solution.py:34
  57.9 2.0 %collective-permute-done.27 = bf16[16,512]{1,0:T(8,128)(2,1)S(1)} collective-permute-done((bf16[16,512]{1,0:T(8,128)(2,1)S(1)}, bf16[16,512]{1,0:T(8,128)(2,1)S(1)}, u32[]{:S(2)}, u32[]{:S(2)}) %collective-permute-start.27) | collective-permute-done | bytes 16416 | tf_op jit(solution)/shard_map/ppermute | solution.py:34
  59.9 0.7 %collective-permute-done.26 = bf16[16,512]{1,0:T(8,128)(2,1)S(1)} collective-permute-done((bf16[16,512]{1,0:T(8,128)(2,1)S(1)}, bf16[16,512]{1,0:T(8,128)(2,1)S(1)}, u32[]{:S(2)}, u32[]{:S(2)}) %collective-permute-start.26) | collective-permute-done | bytes 16416 | tf_op jit(solution)/shard_map/ppermute | solution.py:34
  60.6 0.6 %fusion.6 = bf16[16,512]{1,0:T(8,128)(2,1)} fusion(f32[16,512]{1,0:T(8,128)S(1)} %get-tuple-element.52, f32[64,512]{1,0:T(8,128)S(1)} %get-tuple-element.60, bf16[16,512]{1,0:T(8,128)(2,1)S(1)} %collective-permute-done.27, bf16[16,512]{1,0:T(8,128)(2,1)S(1)} %collective-permute-done.26, bf16[16,512]{1,0:T(8,128)(2,1)S(1)} %collective-permute-done.25), kind=kLoop, calls=%fused_computation.13 | loop fusion | flops 65536 | bytes 131072 | tf_op jit(solution)/shard_map/convert_element_type | solution.py:319
  (41 shorter events, 4.3 us)
Async XLA Ops:
  0.0 0.8 %copy-start = (bf16[16,2048]{1,0:T(8,128)(2,1)S(1)}, bf16[16,2048]{1,0:T(8,128)(2,1)}, u32[]{:S(2)}) copy-start(bf16[16,2048]{1,0:T(8,128)(2,1)} %tokens_ref.1) | copy-start | bytes 196612
  0.8 5.4 %collective-permute-start = (bf16[16,512]{1,0:T(8,128)(2,1)S(1)}, bf16[16,512]{1,0:T(8,128)(2,1)S(1)}, u32[]{:S(2)}, u32[]{:S(2)}) collective-permute-start(bf16[16,512]{1,0:T(8,128)(2,1)S(1)} %get-tuple-element.35), channel_id=1, source_target_pairs={{0,12},{4,8},{8,4},{12,0},{16,28},{20,24},{24,20},{28,16},{1,13},{... | collective-permute-start | bytes 49160 | tf_op jit(solution)/shard_map/ppermute | solution.py:34
  3.3 4.4 %collective-permute-start.1 = (bf16[16,512]{1,0:T(8,128)(2,1)S(1)}, bf16[16,512]{1,0:T(8,128)(2,1)S(1)}, u32[]{:S(2)}, u32[]{:S(2)}) collective-permute-start(bf16[16,512]{1,0:T(8,128)(2,1)S(1)} %get-tuple-element.36), channel_id=1, source_target_pairs={{0,20},{4,16},{8,28},{12,24},{16,4},{20,0},{24,12},{28,8},{1,21},{... | collective-permute-start | bytes 49160 | tf_op jit(solution)/shard_map/ppermute | solution.py:34
  6.2 5.1 %collective-permute-start.2 = (bf16[16,512]{1,0:T(8,128)(2,1)S(1)}, bf16[16,512]{1,0:T(8,128)(2,1)S(1)}, u32[]{:S(2)}, u32[]{:S(2)}) collective-permute-start(bf16[16,512]{1,0:T(8,128)(2,1)S(1)} %get-tuple-element.37), channel_id=1, source_target_pairs={{0,28},{4,24},{8,20},{12,16},{16,12},{20,8},{24,4},{28,0},{1,29},{... | collective-permute-start | bytes 49160 | tf_op jit(solution)/shard_map/ppermute | solution.py:34
  6.2 8.2 %collective-permute-start.3 = (bf16[16,512]{1,0:T(8,128)(2,1)S(1)}, bf16[16,512]{1,0:T(8,128)(2,1)S(1)}, u32[]{:S(2)}, u32[]{:S(2)}) collective-permute-start(bf16[16,512]{1,0:T(8,128)(2,1)S(1)} %get-tuple-element.34.refs_0_), channel_id=1, source_target_pairs={{0,4},{4,0},{8,12},{12,8},{16,20},{20,16},{24,28},{28,24},{1,5},{5... | collective-permute-start | bytes 49160 | tf_op jit(solution)/shard_map/ppermute | solution.py:27
  6.2 8.2 %collective-permute-start.4 = (bf16[16,512]{1,0:T(8,128)(2,1)S(1)}, bf16[16,512]{1,0:T(8,128)(2,1)S(1)}, u32[]{:S(2)}, u32[]{:S(2)}) collective-permute-start(bf16[16,512]{1,0:T(8,128)(2,1)S(1)} %collective-permute-done.refs_1_), channel_id=1, source_target_pairs={{0,4},{4,0},{8,12},{12,8},{16,20},{20,16},{24,28},{28,24},{1,5},{5... | collective-permute-start | bytes 49160 | tf_op jit(solution)/shard_map/ppermute | solution.py:27
  7.7 6.7 %collective-permute-start.5 = (bf16[16,512]{1,0:T(8,128)(2,1)S(1)}, bf16[16,512]{1,0:T(8,128)(2,1)S(1)}, u32[]{:S(2)}, u32[]{:S(2)}) collective-permute-start(bf16[16,512]{1,0:T(8,128)(2,1)S(1)} %collective-permute-done.1.refs_2_), channel_id=1, source_target_pairs={{0,4},{4,0},{8,12},{12,8},{16,20},{20,16},{24,28},{28,24},{1,5},{5... | collective-permute-start | bytes 49160 | tf_op jit(solution)/shard_map/ppermute | solution.py:27
  11.3 3.1 %collective-permute-start.6 = (bf16[16,512]{1,0:T(8,128)(2,1)S(1)}, bf16[16,512]{1,0:T(8,128)(2,1)S(1)}, u32[]{:S(2)}, u32[]{:S(2)}) collective-permute-start(bf16[16,512]{1,0:T(8,128)(2,1)S(1)} %collective-permute-done.2.refs_3_), channel_id=1, source_target_pairs={{0,4},{4,0},{8,12},{12,8},{16,20},{20,16},{24,28},{28,24},{1,5},{5... | collective-permute-start | bytes 49160 | tf_op jit(solution)/shard_map/ppermute | solution.py:27
  14.7 1.4 %collective-permute-start.7 = (bf16[64,896]{1,0:T(8,128)(2,1)S(1)}, bf16[64,896]{1,0:T(8,128)(2,1)S(1)}, u32[]{:S(2)}, u32[]{:S(2)}) collective-permute-start(bf16[64,896]{1,0:T(8,128)(2,1)S(1)} %get-tuple-element.44), channel_id=1, source_target_pairs={{0,4},{4,0},{8,12},{12,8},{16,20},{20,16},{24,28},{28,24},{1,5},{5... | collective-permute-start | bytes 344072 | tf_op jit(solution)/shard_map/ppermute | solution.py:27
  16.2 5.2 %collective-permute-start.10 = (bf16[16,896]{1,0:T(8,128)(2,1)S(1)}, bf16[16,896]{1,0:T(8,128)(2,1)S(1)}, u32[]{:S(2)}, u32[]{:S(2)}) collective-permute-start(bf16[16,896]{1,0:T(8,128)(2,1)S(1)} %get-tuple-element.68), channel_id=1, source_target_pairs={{0,28},{4,24},{8,20},{12,16},{16,12},{20,8},{24,4},{28,0},{1,29},{... | collective-permute-start | bytes 86024 | tf_op jit(solution)/shard_map/ppermute | solution.py:34
  16.3 5.1 %collective-permute-start.9 = (bf16[16,896]{1,0:T(8,128)(2,1)S(1)}, bf16[16,896]{1,0:T(8,128)(2,1)S(1)}, u32[]{:S(2)}, u32[]{:S(2)}) collective-permute-start(bf16[16,896]{1,0:T(8,128)(2,1)S(1)} %get-tuple-element.69), channel_id=1, source_target_pairs={{0,20},{4,16},{8,28},{12,24},{16,4},{20,0},{24,12},{28,8},{1,21},{... | collective-permute-start | bytes 86024 | tf_op jit(solution)/shard_map/ppermute | solution.py:34
  16.3 5.9 %collective-permute-start.8 = (bf16[16,896]{1,0:T(8,128)(2,1)S(1)}, bf16[16,896]{1,0:T(8,128)(2,1)S(1)}, u32[]{:S(2)}, u32[]{:S(2)}) collective-permute-start(bf16[16,896]{1,0:T(8,128)(2,1)S(1)} %get-tuple-element.70), channel_id=1, source_target_pairs={{0,12},{4,8},{8,4},{12,0},{16,28},{20,24},{24,20},{28,16},{1,13},{... | collective-permute-start | bytes 86024 | tf_op jit(solution)/shard_map/ppermute | solution.py:34
  23.3 5.2 %collective-permute-start.13 = (bf16[16,2048]{1,0:T(8,128)(2,1)S(1)}, bf16[16,2048]{1,0:T(8,128)(2,1)S(1)}, u32[]{:S(2)}, u32[]{:S(2)}) collective-permute-start(bf16[16,2048]{1,0:T(8,128)(2,1)S(1)} %recurrent.1.part_ref), channel_id=1, source_target_pairs={{0,3},{1,2},{2,1},{3,0},{4,7},{5,6},{6,5},{7,4},{8,11},{9,10},{10,... | collective-permute-start | bytes 196616 | tf_op jit(solution)/shard_map/ppermute | solution.py:47
  25.7 4.3 %collective-permute-start.12 = (bf16[16,2048]{1,0:T(8,128)(2,1)S(1)}, bf16[16,2048]{1,0:T(8,128)(2,1)S(1)}, u32[]{:S(2)}, u32[]{:S(2)}) collective-permute-start(bf16[16,2048]{1,0:T(8,128)(2,1)S(1)} %recurrent.1.part_ref), channel_id=1, source_target_pairs={{0,2},{1,3},{2,0},{3,1},{4,6},{5,7},{6,4},{7,5},{8,10},{9,11},{10,... | collective-permute-start | bytes 196616 | tf_op jit(solution)/shard_map/ppermute | solution.py:47
  26.2 4.3 %collective-permute-start.11 = (bf16[16,2048]{1,0:T(8,128)(2,1)S(1)}, bf16[16,2048]{1,0:T(8,128)(2,1)S(1)}, u32[]{:S(2)}, u32[]{:S(2)}) collective-permute-start(bf16[16,2048]{1,0:T(8,128)(2,1)S(1)} %recurrent.1.part_ref), channel_id=1, source_target_pairs={{0,1},{1,0},{2,3},{3,2},{4,5},{5,4},{6,7},{7,6},{8,9},{9,8},{10,11... | collective-permute-start | bytes 196616 | tf_op jit(solution)/shard_map/ppermute | solution.py:47
  30.7 6.3 %collective-permute-start.16 = (bf16[16,2176]{1,0:T(8,128)(2,1)S(1)}, bf16[16,2176]{1,0:T(8,128)(2,1)S(1)}, u32[]{:S(2)}, u32[]{:S(2)}) collective-permute-start(bf16[16,2176]{1,0:T(8,128)(2,1)S(1)} %get-tuple-element.53.refs_0_), channel_id=1, source_target_pairs={{0,28},{4,24},{8,20},{12,16},{16,12},{20,8},{24,4},{28,0},{1,29},{... | collective-permute-start | bytes 208904 | tf_op jit(solution)/shard_map/ppermute | solution.py:34
  30.8 8.8 %collective-permute-start.15 = (bf16[16,2176]{1,0:T(8,128)(2,1)S(1)}, bf16[16,2176]{1,0:T(8,128)(2,1)S(1)}, u32[]{:S(2)}, u32[]{:S(2)}) collective-permute-start(bf16[16,2176]{1,0:T(8,128)(2,1)S(1)} %get-tuple-element.53.refs_0_), channel_id=1, source_target_pairs={{0,20},{4,16},{8,28},{12,24},{16,4},{20,0},{24,12},{28,8},{1,21},{... | collective-permute-start | bytes 208904 | tf_op jit(solution)/shard_map/ppermute | solution.py:34
  33.3 6.3 %collective-permute-start.14 = (bf16[16,2176]{1,0:T(8,128)(2,1)S(1)}, bf16[16,2176]{1,0:T(8,128)(2,1)S(1)}, u32[]{:S(2)}, u32[]{:S(2)}) collective-permute-start(bf16[16,2176]{1,0:T(8,128)(2,1)S(1)} %get-tuple-element.53.refs_0_), channel_id=1, source_target_pairs={{0,12},{4,8},{8,4},{12,0},{16,28},{20,24},{24,20},{28,16},{1,13},{... | collective-permute-start | bytes 208904 | tf_op jit(solution)/shard_map/ppermute | solution.py:34
  33.3 9.7 %collective-permute-start.17 = (bf16[16,2176]{1,0:T(8,128)(2,1)S(1)}, bf16[16,2176]{1,0:T(8,128)(2,1)S(1)}, u32[]{:S(2)}, u32[]{:S(2)}) collective-permute-start(bf16[16,2176]{1,0:T(8,128)(2,1)S(1)} %get-tuple-element.53.refs_0_), channel_id=1, source_target_pairs={{0,4},{4,0},{8,12},{12,8},{16,20},{20,16},{24,28},{28,24},{1,5},{5... | collective-permute-start | bytes 208904 | tf_op jit(solution)/shard_map/ppermute | solution.py:27
  37.0 6.0 %collective-permute-start.20 = (bf16[16,2176]{1,0:T(8,128)(2,1)S(1)}, bf16[16,2176]{1,0:T(8,128)(2,1)S(1)}, u32[]{:S(2)}, u32[]{:S(2)}) collective-permute-start(bf16[16,2176]{1,0:T(8,128)(2,1)S(1)} %collective-permute-done.16.refs_3_), channel_id=1, source_target_pairs={{0,4},{4,0},{8,12},{12,8},{16,20},{20,16},{24,28},{28,24},{1,5},{5... | collective-permute-start | bytes 208904 | tf_op jit(solution)/shard_map/ppermute | solution.py:27
  39.6 3.4 %collective-permute-start.19 = (bf16[16,2176]{1,0:T(8,128)(2,1)S(1)}, bf16[16,2176]{1,0:T(8,128)(2,1)S(1)}, u32[]{:S(2)}, u32[]{:S(2)}) collective-permute-start(bf16[16,2176]{1,0:T(8,128)(2,1)S(1)} %collective-permute-done.15.refs_2_), channel_id=1, source_target_pairs={{0,4},{4,0},{8,12},{12,8},{16,20},{20,16},{24,28},{28,24},{1,5},{5... | collective-permute-start | bytes 208904 | tf_op jit(solution)/shard_map/ppermute | solution.py:27
  39.6 3.4 %collective-permute-start.18 = (bf16[16,2176]{1,0:T(8,128)(2,1)S(1)}, bf16[16,2176]{1,0:T(8,128)(2,1)S(1)}, u32[]{:S(2)}, u32[]{:S(2)}) collective-permute-start(bf16[16,2176]{1,0:T(8,128)(2,1)S(1)} %collective-permute-done.14.refs_1_), channel_id=1, source_target_pairs={{0,4},{4,0},{8,12},{12,8},{16,20},{20,16},{24,28},{28,24},{1,5},{5... | collective-permute-start | bytes 208904 | tf_op jit(solution)/shard_map/ppermute | solution.py:27
  44.2 1.6 %collective-permute-start.21 = (bf16[4,64,512]{2,1,0:T(8,128)(2,1)S(1)}, bf16[4,64,512]{2,1,0:T(8,128)(2,1)S(1)}, u32[]{:S(2)}, u32[]{:S(2)}) collective-permute-start(bf16[4,64,512]{2,1,0:T(8,128)(2,1)S(1)} %get-tuple-element.58), channel_id=1, source_target_pairs={{0,4},{4,0},{8,12},{12,8},{16,20},{20,16},{24,28},{28,24},{1,5},{5... | collective-permute-start | bytes 786440 | tf_op jit(solution)/shard_map/ppermute | solution.py:27
  45.9 4.1 %collective-permute-start.22 = (bf16[64,512]{1,0:T(8,128)(2,1)S(1)}, bf16[64,512]{1,0:T(8,128)(2,1)S(1)}, u32[]{:S(2)}, u32[]{:S(2)}) collective-permute-start(bf16[64,512]{1,0:T(8,128)(2,1)S(1)} %get-tuple-element.65), channel_id=1, source_target_pairs={{0,5},{1,4},{2,7},{3,6},{4,1},{5,0},{6,3},{7,2},{8,13},{9,12},{10,... | collective-permute-start | bytes 196616 | tf_op jit(solution)/shard_map/ppermute | solution.py:47
  47.4 5.6 %collective-permute-start.24 = (bf16[64,512]{1,0:T(8,128)(2,1)S(1)}, bf16[64,512]{1,0:T(8,128)(2,1)S(1)}, u32[]{:S(2)}, u32[]{:S(2)}) collective-permute-start(bf16[64,512]{1,0:T(8,128)(2,1)S(1)} %get-tuple-element.66), channel_id=1, source_target_pairs={{0,7},{1,6},{2,5},{3,4},{4,3},{5,2},{6,1},{7,0},{8,15},{9,14},{10,... | collective-permute-start | bytes 196616 | tf_op jit(solution)/shard_map/ppermute | solution.py:47
  49.2 5.4 %collective-permute-start.23 = (bf16[64,512]{1,0:T(8,128)(2,1)S(1)}, bf16[64,512]{1,0:T(8,128)(2,1)S(1)}, u32[]{:S(2)}, u32[]{:S(2)}) collective-permute-start(bf16[64,512]{1,0:T(8,128)(2,1)S(1)} %get-tuple-element.67), channel_id=1, source_target_pairs={{0,6},{1,7},{2,4},{3,5},{4,2},{5,3},{6,0},{7,1},{8,14},{9,15},{10,... | collective-permute-start | bytes 196616 | tf_op jit(solution)/shard_map/ppermute | solution.py:47
  54.7 3.2 %collective-permute-start.25 = (bf16[16,512]{1,0:T(8,128)(2,1)S(1)}, bf16[16,512]{1,0:T(8,128)(2,1)S(1)}, u32[]{:S(2)}, u32[]{:S(2)}) collective-permute-start(bf16[16,512]{1,0:T(8,128)(2,1)S(1)} %get-tuple-element.71), channel_id=1, source_target_pairs={{0,12},{4,8},{8,4},{12,0},{16,28},{20,24},{24,20},{28,16},{1,13},{... | collective-permute-start | bytes 49160 | tf_op jit(solution)/shard_map/ppermute | solution.py:34
  54.8 5.1 %collective-permute-start.27 = (bf16[16,512]{1,0:T(8,128)(2,1)S(1)}, bf16[16,512]{1,0:T(8,128)(2,1)S(1)}, u32[]{:S(2)}, u32[]{:S(2)}) collective-permute-start(bf16[16,512]{1,0:T(8,128)(2,1)S(1)} %get-tuple-element.72), channel_id=1, source_target_pairs={{0,28},{4,24},{8,20},{12,16},{16,12},{20,8},{24,4},{28,0},{1,29},{... | collective-permute-start | bytes 49160 | tf_op jit(solution)/shard_map/ppermute | solution.py:34
  55.7 4.9 %collective-permute-start.26 = (bf16[16,512]{1,0:T(8,128)(2,1)S(1)}, bf16[16,512]{1,0:T(8,128)(2,1)S(1)}, u32[]{:S(2)}, u32[]{:S(2)}) collective-permute-start(bf16[16,512]{1,0:T(8,128)(2,1)S(1)} %get-tuple-element.73), channel_id=1, source_target_pairs={{0,20},{4,16},{8,28},{12,24},{16,4},{20,0},{24,12},{28,8},{1,21},{... | collective-permute-start | bytes 49160 | tf_op jit(solution)/shard_map/ppermute | solution.py:34
where the time goes:
time: 61.4 us; the launch traced here: 61.2 us
  starting transfers between devices  25.6 us (42%)
  waiting for transfers between devices  25.4 us (41%)
  Pallas kernels  8.33 us (14%)
  local copies, waits for them, and re-layouts  0.87 us (1%)
  other arithmetic  0.76 us (1%)
    ppermute x12, starting transfers between devices, swap_chips(): lax.ppermute(blocks[k], 'ep', [(i, i ^ 2 * k + 1) for i in range(count)])  15.1 us
    ppermute x12, waiting for transfers between devices, swap_chips(): lax.ppermute(blocks[k], 'ep', [(i, i ^ 2 * k + 1) for i in range(count)])  13.8 us
    ppermute x6, waiting for transfers between devices, swap_heads(): got[k] = lax.ppermute(blocks[k], ('ep', 'tp'), pairs)  9.15 us
    ppermute x6, starting transfers between devices, swap_heads(): got[k] = lax.ppermute(blocks[k], ('ep', 'tp'), pairs)  6.81 us
    pallas_call x2, Pallas kernels, load_call(): pl.pallas_call(functools.partial(kernel, len(args)), out_shape=tuple(outs...  5.84 us
    ppermute x10, starting transfers between devices, swap_core(): return lax.ppermute(block, 'ep', [(i, i ^ 1) for i in range(count)])  3.72 us
    ppermute x10, waiting for transfers between devices, swap_core(): return lax.ppermute(block, 'ep', [(i, i ^ 1) for i in range(count)])  2.51 us
    pallas_call x4, Pallas kernels, call(): pl.pallas_call(kernel, out_shape=tuple(outs), in_specs=[pl.BlockSpec(memo...  1.52 us
  transfers between devices with their start and end apart: 28, of which 17 were waited for; matrix products, arithmetic and copies ran while one was open for 0% of the time, Pallas kernels for 10%

commit v1 on v0

--- a/solution.py
+++ b/solution.py
@@ -61,28 +61,21 @@
     )(*args)
 
 
-def load_call(kernel, args, extra):
-    outs = [like(a.shape, a.dtype) for a in args] + list(extra)
+def load_call(kernel, args, outs, copies, near=()):
     return pl.pallas_call(
-        functools.partial(kernel, len(args)),
+        kernel,
         out_shape=tuple(outs),
-        in_specs=[pl.BlockSpec(memory_space=pltpu.HBM)] * len(args),
+        in_specs=[pl.BlockSpec(memory_space=pltpu.VMEM)] * len(near)
+        + [pl.BlockSpec(memory_space=pltpu.HBM)] * len(args),
         out_specs=tuple(pl.BlockSpec(memory_space=pltpu.VMEM) for _ in outs),
-        scratch_shapes=[pltpu.SemaphoreType.DMA((len(args),))],
+        scratch_shapes=[pltpu.SemaphoreType.DMA((copies,))],
         compiler_params=pltpu.CompilerParams(vmem_limit_bytes=2 << 20),
         cost_estimate=pl.CostEstimate(flops=1 << 22, bytes_accessed=1 << 22, transcendentals=0),
-    )(*[pltpu.with_memory_space_constraint(a, pltpu.HBM) for a in args])
+    )(*near, *[pltpu.with_memory_space_constraint(a, pltpu.HBM) for a in args])
 
 
 def like(shape, dtype):
     return jax.ShapeDtypeStruct(shape, dtype)
-
-
-def spread_kernel(tokens_ref, *out_refs):
-    chip = lax.axis_index("ep") // 2
-    cols = out_refs[0].shape[1]
-    for k, out in enumerate(out_refs):
-        out[...] = tokens_ref[:, pl.ds(pl.multiple_of((chip ^ k) * cols, lane_tile), cols)]
 
 
 def load(pairs, sems):
@@ -97,15 +90,34 @@
         copy.wait()
 
 
+def spread_kernel(weights, *refs):
+    tokens_ref, weight_refs, refs = refs[0], refs[1 : 1 + weights], refs[1 + weights :]
+    *block_refs, near_ref, joined_ref, sems = refs
+    chip = lax.axis_index("ep") // 2
+    cols = block_refs[0].shape[1]
+    pairs = []
+    for k in range(len(block_refs) - 1, -1, -1):
+        at = pl.ds(pl.multiple_of((chip ^ k) * cols, lane_tile), cols)
+        pairs.append((tokens_ref.at[:, at], block_refs[k]))
+    pairs.append((tokens_ref, near_ref))
+    at = 0
+    for weight in weight_refs:
+        pairs.append((weight, joined_ref.at[:, at : at + weight.shape[1]]))
+        at += weight.shape[1]
+    for copy in load(pairs, sems):
+        copy.wait()
+
+
 def side_kernel(count, *refs):
+    tokens_ref, refs = refs[0], refs[1:]
     loaded = refs[count : 2 * count]
     scale_ref, share_ref, sems = refs[2 * count :]
     copies = load(list(zip(refs[:count], loaded)), sems)
-    for copy in copies[:4]:
+    scale_ref[...] = jnp.broadcast_to(inverse_rms(tokens_ref[...].astype(wide)), scale_ref.shape)
+    for copy in copies[:3]:
         copy.wait()
-    tokens_ref, ids_ref, group_ref, inner_ref = loaded[:4]
+    ids_ref, group_ref, inner_ref = loaded[:3]
     experts = lax.axis_size("ep")
-    scale_ref[...] = jnp.broadcast_to(inverse_rms(tokens_ref[...].astype(wide)), scale_ref.shape)
     lanes, seqs = share_ref.shape[1], share_ref.shape[0]
     inner = inner_ref[...]
     weight = group_ref[...] * inner / jnp.sum(inner, axis=0, keepdims=True)
@@ -117,27 +129,25 @@
     high = share.astype(narrow).astype(wide)
     packed = jnp.where(place < experts, high, jnp.where(place < 2 * experts, share - high, 0.0))
     share_ref[...] = packed.T.astype(narrow)
-    for copy in copies[4:]:
+    for copy in copies[3:]:
         copy.wait()
 
 
 def project_kernel(chips, gain_ref, *refs):
-    blocks, refs = refs[: 2 * chips], refs[2 * chips :]
-    weights, (own_ref, away_ref) = refs[:-2], refs[-2:]
+    blocks, (own_ref, other_ref), outs = refs[:chips], refs[chips : chips + 2], refs[chips + 2 :]
     me = lax.axis_index("ep")
-    south = me % 2 == 0
-    feats = weights[0].shape[0]
+    first = me % 2 == 0
+    feats = own_ref.shape[0]
     pair_gain = gain_ref[:, pl.ds(pl.multiple_of(me // 2 * 2 * feats, lane_tile), 2 * feats)]
     rows = jnp.concatenate([block[...] for block in blocks], axis=0).astype(wide) * pair_gain
-    rows = jnp.where(south, rows[:, :feats], rows[:, feats:]).astype(narrow)
-    half = own_ref.shape[0]
-    at = 0
-    for weight in weights:
-        cols = weight.shape[1]
-        product = jnp.dot(rows, weight[...], preferred_element_type=wide)
-        own_ref[:, at : at + cols] = product[:half]
-        away_ref[:, at : at + cols] = product[half:].astype(narrow)
-        at += cols
+    low, high = rows[:, :feats], rows[:, feats:]
+    mine = jnp.where(first, low, high).astype(narrow)
+    others = jnp.where(first, high, low).astype(narrow)
+    product = jnp.dot(mine, own_ref[...], preferred_element_type=wide)
+    product = product + jnp.dot(others, other_ref[...], preferred_element_type=wide)
+    seqs = outs[0].shape[0]
+    for k, out in enumerate(outs):
+        out[...] = product[k * seqs : (k + 1) * seqs].astype(out.dtype)
 
 
 def recurrent_kernel(chips, cuts, base_ref, *refs):
@@ -193,25 +203,30 @@
 
 
 def expert_kernel(count, *refs):
-    blocks, (gate_ref, up_ref, down_ref, own_ref, away_ref) = refs[:count], refs[count:]
-    width = gate_ref.shape[1]
+    blocks, weights, outs = refs[:count], refs[count : count + 6], refs[count + 6 :]
+    width = weights[0].shape[1]
     rows = jnp.concatenate([block[:, :width] for block in blocks], axis=0)
     share = jnp.concatenate([block[:, width:] for block in blocks], axis=0).astype(wide)
     me, experts = lax.axis_index("ep"), lax.axis_size("ep")
+    head = lax.axis_index("tp")
     place = lax.broadcasted_iota(jnp.int32, share.shape, 1)
-    chosen = (place == me) | (place == me + experts)
-    weight = jnp.sum(jnp.where(chosen, share, 0.0), axis=1, keepdims=True)
-    gate = jnp.dot(rows, gate_ref[0], preferred_element_type=wide)
-    upper = jnp.dot(rows, up_ref[0], preferred_element_type=wide)
-    hidden = (silu(gate) * upper).astype(narrow)
-    head = lax.axis_index("tp")
-    pieces, half, cols = own_ref.shape
-    for k in range(pieces):
+    hiddens, factors = [], []
+    for n in range(2):
+        gate_ref, up_ref = weights[3 * n], weights[3 * n + 1]
+        chosen = (place == me ^ n) | (place == (me ^ n) + experts)
+        factors.append(jnp.sum(jnp.where(chosen, share, 0.0), axis=1, keepdims=True))
+        gate = jnp.dot(rows, gate_ref[0], preferred_element_type=wide)
+        upper = jnp.dot(rows, up_ref[0], preferred_element_type=wide)
+        hiddens.append((silu(gate) * upper).astype(narrow))
+    cols = outs[0].shape[1]
+    for k, out in enumerate(outs):
         at = pl.ds(pl.multiple_of((head ^ k) * cols, lane_tile), cols)
-        out = jnp.dot(hidden, down_ref[0, :, at], preferred_element_type=wide) * weight
-        near, far = (out[:half], out[half:]) if k == 0 else (out[half:], out[:half])
-        own_ref[k] = near
-        away_ref[k] = far.astype(narrow)
+        total = None
+        for n in range(2):
+            down_ref = weights[3 * n + 2]
+            part = jnp.dot(hiddens[n], down_ref[0, :, at], preferred_element_type=wide) * factors[n]
+            total = part if total is None else total + part
+        out[...] = total.astype(out.dtype)
 
 
 def on_device(
@@ -246,20 +261,21 @@
     lanes = -(-2 * ep_count // lane_tile) * lane_tile
     mib = 1 << 20
 
-    pair_cols = call(spread_kernel, [like((seqs, 2 * feats), narrow)] * chips, (tokens,), 4 * mib)
+    weights = (w_query, w_key, w_decay, w_value, w_outgate)
+    *pair_cols, tokens_near, joined = load_call(
+        functools.partial(spread_kernel, len(weights)),
+        (tokens, *weights),
+        [like((seqs, 2 * feats), narrow)] * chips
+        + [like(tokens.shape, narrow), like((feats, proj_cols), narrow)],
+        chips + 1 + len(weights),
+    )
     blocks = [pair_cols[0], *swap_chips(pair_cols)]
-    blocks += [swap_core(block) for block in blocks]
+    joined_other = swap_core(joined)
     side_args = (
-        tokens,
         expert_ids.T,
         group_prob[None, :],
         inner_prob.T,
         norm_gain[None, :],
-        w_query,
-        w_key,
-        w_decay,
-        w_value,
-        w_outgate,
         decay_rate[None, :],
         head_gain[None, :],
         moe_gain[None, :],
@@ -267,21 +283,31 @@
         state,
     )
     loaded = load_call(
-        side_kernel, side_args, [like((seqs, lane_tile), wide), like((seqs, lanes), narrow)]
-    )
-    tokens_near = loaded[0]
-    gain, weights = loaded[4], loaded[5:10]
-    rate, read_gain, mix_gain, output_near, state_near, scale, share = loaded[10:]
-    own, away = call(
+        functools.partial(side_kernel, len(side_args)),
+        side_args,
+        [like(a.shape, a.dtype) for a in side_args]
+        + [like((seqs, lane_tile), wide), like((seqs, lanes), narrow)],
+        len(side_args),
+        near=(tokens_near,),
+    )
+    gain, rate, read_gain, mix_gain, output_near, state_near, scale, share = loaded[3:]
+    base, *sums = call(
         functools.partial(project_kernel, chips),
-        [like((half, proj_cols), wide), like((half, proj_cols), narrow)],
-        (gain, *blocks, *weights),
+        [like((seqs, proj_cols), wide)] + [like((seqs, proj_cols), narrow)] * (chips - 1),
+        (gain, *blocks, joined, joined_other),
         8 * mib,
     )
-    both = own + swap_core(away).astype(wide)
-    both_narrow = both.astype(narrow)
-    arrived = swap_chips([both_narrow[k * seqs : (k + 1) * seqs] for k in range(chips)])
-    expert_weights = load_call(load_kernel, (w_gate, w_up, w_down), [])
+    arrived = swap_chips([base, *sums])
+    expert_weights = (w_gate, w_up, w_down)
+    expert_weights = load_call(
+        functools.partial(load_kernel, 3),
+        expert_weights,
+        [like(a.shape, a.dtype) for a in expert_weights],
+        3,
+    )
+    other_weights = []
+    for weight in expert_weights:
+        other_weights.append(swap_core(weight))
     (part,) = pl.pallas_call(
         functools.partial(recurrent_kernel, chips, (query_cols, value_cols)),
         out_shape=(like((seqs, width), narrow),),
@@ -291,7 +317,7 @@
         compiler_params=pltpu.CompilerParams(vmem_limit_bytes=8 * mib),
         cost_estimate=pl.CostEstimate(flops=1 << 20, bytes_accessed=4 << 20, transcendentals=0),
         name="recurrent",
-    )(both[:seqs], *arrived, scale, rate, state_near, read_gain, output_near)
+    )(base, *arrived, scale, rate, state_near, read_gain, output_near)
     parts = swap_heads([part] * tp_count, 0)
     sending, mixed_own = call(
         functools.partial(mix_kernel, tp_count - 1),
@@ -300,17 +326,13 @@
         4 * mib,
     )
     rows = [sending, *swap_chips([sending] * chips)]
-    rows += [swap_core(block) for block in rows]
-    own, away = call(
-        functools.partial(expert_kernel, 2 * chips),
-        [like((tp_count, half, cols), wide), like((tp_count, half, cols), narrow)],
-        (*rows, *expert_weights),
+    head_sum, *pieces = call(
+        functools.partial(expert_kernel, chips),
+        [like((half, cols), wide)] + [like((half, cols), narrow)] * (tp_count - 1),
+        (*rows, *expert_weights, *other_weights),
         24 * mib,
     )
-    pair_sum = own + swap_core(away).astype(wide)
-    pair_narrow = pair_sum.astype(narrow)
-    head_sum = pair_sum[0]
-    for block in swap_heads([pair_narrow[k] for k in range(tp_count)], 1):
+    for block in swap_heads([head_sum, *pieces], 0):
         head_sum = head_sum + block.astype(wide)
     head_narrow = head_sum.astype(narrow)
     moe_sum = head_sum[:seqs]

time: 61.4 us -> 66.9 us (1.090)
  waiting for transfers between devices: 25.4 us -> 29 us
  Pallas kernels: 8.33 us -> 10.5 us
  local copies, waits for them, and re-layouts: 0.87 us -> 0.01 us
    ppermute x12, waiting for transfers between devices: 13.8 us -> 19.2 us  [swap_chips(): lax.ppermute(blocks[k], 'ep', [(i, i ^ 2 * k + 1) for i in range(count)])]
    ppermute x10 -> x4, starting transfers between devices: 3.72 us -> 1.21 us  [swap_core(): return lax.ppermute(block, 'ep', [(i, i ^ 1) for i in range(count)])]
    ppermute x10 -> x4, waiting for transfers between devices: 2.51 us -> 0.01 us  [swap_core(): return lax.ppermute(block, 'ep', [(i, i ^ 1) for i in range(count)])]
    ppermute x12, starting transfers between devices: 15.1 us -> 16.7 us  [swap_chips(): lax.ppermute(blocks[k], 'ep', [(i, i ^ 2 * k + 1) for i in range(count)])]
    ppermute x6, starting transfers between devices: 6.81 us -> 8.12 us  [swap_heads(): got[k] = lax.ppermute(blocks[k], ('ep', 'tp'), pairs)]
    pallas_call x4 -> x3, Pallas kernels: 1.52 us -> 2.76 us  [call(): pl.pallas_call(kernel, out_shape=tuple(outs), in_specs=[pl.BlockSpec(memo...]
    pallas_call x2 -> x3, Pallas kernels: 5.84 us -> 6.81 us  [load_call(): pl.pallas_call(kernel, out_shape=tuple(outs), in_specs=[pl.BlockSpec(memo...]
    unnamed x2 -> x0, local copies, waits for them, and re-layouts: 0.84 us -> none
  transfers between devices with their start and end apart: 28 -> 22, of which waited for: 17 -> 14; matrix products, arithmetic and copies ran while one was open for 0% -> 0% of each run, Pallas kernels for 10% -> 8%
where the time goes in v1:
time: 66.9 us; the launch traced here: 66.3 us
  waiting for transfers between devices  29 us (43%)
  starting transfers between devices  26 us (39%)
  Pallas kernels  10.5 us (16%)
    ppermute x12, waiting for transfers between devices, swap_chips(): lax.ppermute(blocks[k], 'ep', [(i, i ^ 2 * k + 1) for i in range(count)])  19.2 us
    ppermute x12, starting transfers between devices, swap_chips(): lax.ppermute(blocks[k], 'ep', [(i, i ^ 2 * k + 1) for i in range(count)])  16.7 us
    ppermute x6, waiting for transfers between devices, swap_heads(): got[k] = lax.ppermute(blocks[k], ('ep', 'tp'), pairs)  9.7 us
    ppermute x6, starting transfers between devices, swap_heads(): got[k] = lax.ppermute(blocks[k], ('ep', 'tp'), pairs)  8.12 us
    pallas_call x3, Pallas kernels, load_call(): pl.pallas_call(kernel, out_shape=tuple(outs), in_specs=[pl.BlockSpec(memo...  6.81 us
    pallas_call x3, Pallas kernels, call(): pl.pallas_call(kernel, out_shape=tuple(outs), in_specs=[pl.BlockSpec(memo...  2.76 us
  transfers between devices with their start and end apart: 22, of which 14 were waited for; matrix products, arithmetic and copies ran while one was open for 0% of the time, Pallas kernels for 8%

profile of v1, /device:TPU:0, one launch (start us, length us, event | category | flops | bytes accessed | tf_op | source)
XLA Modules:
  0.0 66.3 jit_solution(15774241380795327486)
XLA Ops:
  0.0 2.9 %shard_map.176 = (bf16[1,2048,512]{2,1,0:T(8,128)(2,1)S(1)}, bf16[1,2048,512]{2,1,0:T(8,128)(2,1)S(1)}, bf16[1,512,2048]{2,1,0:T(8,128)(2,1)S(1)}) custom-call(bf16[1,2048,512]{2,1,0:T(8,128)(2,1)} %refs_0_.3, bf16[1,2048,512]{2,1,0:T(8,128)(2,1)} %refs_1_.3, bf16[1,512,2048]{2,1,0:T(8,128)(2,1)} %refs_2_.3), custom_call_target="tpu_custom_call" | custom-call | flops 4194304 | bytes 4194304 | tf_op jit(solution)/shard_map/pallas_call | solution.py:65
  2.9 0.6 collective-permute-start.13
  4.0 1.2 %shard_map.172 = (bf16[16,512]{1,0:T(8,128)(2,1)S(1)}, bf16[16,512]{1,0:T(8,128)(2,1)S(1)}, bf16[16,512]{1,0:T(8,128)(2,1)S(1)}, bf16[16,512]{1,0:T(8,128)(2,1)S...) custom-call(bf16[16,2048]{1,0:T(8,128)(2,1)} %refs_0_.2, bf16[256,128]{1,0:T(8,128)(2,1)} %refs_1_.2, ...), custom_call_target="tpu_custom_call" | custom-call | flops 4194304 | bytes 4194304 | tf_op jit(solution)/shard_map/pallas_call | solution.py:65
  5.4 2.7 %collective-permute-start = (bf16[16,512]{1,0:T(8,128)(2,1)S(1)}, bf16[16,512]{1,0:T(8,128)(2,1)S(1)}, u32[]{:S(2)}, u32[]{:S(2)}) collective-permute-start(bf16[16,512]{1,0:T(8,128)(2,1)S(1)} %get-tuple-element.35), channel_id=1, source_target_pairs={{0,12},{4,8},{8,4},{12,0},{16,28},{20,24},{24,20},{28,16},{1,13},{... | collective-permute-start | bytes 49160 | tf_op jit(solution)/shard_map/ppermute | solution.py:34
  8.0 1.4 %collective-permute-done.refs_1_ = bf16[16,512]{1,0:T(8,128)(2,1)S(1)} collective-permute-done((bf16[16,512]{1,0:T(8,128)(2,1)S(1)}, bf16[16,512]{1,0:T(8,128)(2,1)S(1)}, u32[]{:S(2)}, u32[]{:S(2)}) %collective-permute-start) | collective-permute-done | bytes 16416 | tf_op jit(solution)/shard_map/ppermute | solution.py:34
  9.5 2.8 %collective-permute-start.1 = (bf16[16,512]{1,0:T(8,128)(2,1)S(1)}, bf16[16,512]{1,0:T(8,128)(2,1)S(1)}, u32[]{:S(2)}, u32[]{:S(2)}) collective-permute-start(bf16[16,512]{1,0:T(8,128)(2,1)S(1)} %get-tuple-element.36), channel_id=1, source_target_pairs={{0,20},{4,16},{8,28},{12,24},{16,4},{20,0},{24,12},{28,8},{1,21},{... | collective-permute-start | bytes 49160 | tf_op jit(solution)/shard_map/ppermute | solution.py:34
  12.2 1.4 %collective-permute-done.1.refs_2_ = bf16[16,512]{1,0:T(8,128)(2,1)S(1)} collective-permute-done((bf16[16,512]{1,0:T(8,128)(2,1)S(1)}, bf16[16,512]{1,0:T(8,128)(2,1)S(1)}, u32[]{:S(2)}, u32[]{:S(2)}) %collective-permute-start.1) | collective-permute-done | bytes 16416 | tf_op jit(solution)/shard_map/ppermute | solution.py:34
  13.7 3.9 %collective-permute-start.2 = (bf16[16,512]{1,0:T(8,128)(2,1)S(1)}, bf16[16,512]{1,0:T(8,128)(2,1)S(1)}, u32[]{:S(2)}, u32[]{:S(2)}) collective-permute-start(bf16[16,512]{1,0:T(8,128)(2,1)S(1)} %get-tuple-element.37), channel_id=1, source_target_pairs={{0,28},{4,24},{8,20},{12,16},{16,12},{20,8},{24,4},{28,0},{1,29},{... | collective-permute-start | bytes 49160 | tf_op jit(solution)/shard_map/ppermute | solution.py:34
  17.6 2.7 %shard_map.173 = (s32[2,16]{1,0:T(2,128)}, f32[1,16]{1,0:T(1,128)}, f32[2,16]{1,0:T(2,128)}, f32[1,2048]{1,0:T(1,128)S(1)}, f32[1,128]{1,0:T(1,128)S(1)}, /*inde...) custom-call(bf16[16,2048]{1,0:T(8,128)(2,1)S(1)} %get-tuple-element., ...), custom_call_target="tpu_custom_call" | custom-call | flops 4194304 | bytes 4194304 | tf_op jit(solution)/shard_map/pallas_call | solution.py:65
  20.7 2.8 %collective-permute-start.5 = (bf16[16,896]{1,0:T(8,128)(2,1)S(1)}, bf16[16,896]{1,0:T(8,128)(2,1)S(1)}, u32[]{:S(2)}, u32[]{:S(2)}) collective-permute-start(bf16[16,896]{1,0:T(8,128)(2,1)S(1)} %get-tuple-element.41), channel_id=1, source_target_pairs={{0,20},{4,16},{8,28},{12,24},{16,4},{20,0},{24,12},{28,8},{1,21},{... | collective-permute-start | bytes 86024 | tf_op jit(solution)/shard_map/ppermute | solution.py:34
  24.0 2.3 %collective-permute-start.6 = (bf16[16,896]{1,0:T(8,128)(2,1)S(1)}, bf16[16,896]{1,0:T(8,128)(2,1)S(1)}, u32[]{:S(2)}, u32[]{:S(2)}) collective-permute-start(bf16[16,896]{1,0:T(8,128)(2,1)S(1)} %get-tuple-element.42), channel_id=1, source_target_pairs={{0,28},{4,24},{8,20},{12,16},{16,12},{20,8},{24,4},{28,0},{1,29},{... | collective-permute-start | bytes 86024 | tf_op jit(solution)/shard_map/ppermute | solution.py:34
  26.2 2.8 %collective-permute-done.6.refs_2_ = bf16[16,896]{1,0:T(8,128)(2,1)S(1)} collective-permute-done((bf16[16,896]{1,0:T(8,128)(2,1)S(1)}, bf16[16,896]{1,0:T(8,128)(2,1)S(1)}, u32[]{:S(2)}, u32[]{:S(2)}) %collective-permute-start.6) | collective-permute-done | bytes 28704 | tf_op jit(solution)/shard_map/ppermute | solution.py:34
  29.1 0.9 %recurrent.1.part_ref = bf16[16,2048]{1,0:T(8,128)(2,1)S(1)} custom-call(f32[16,896]{1,0:T(8,128)S(1)} %get-tuple-element.39.base_ref, bf16[16,896]{1,0:T(8,128)(2,1)S(1)} %collective-permute-done.4.refs_0_, bf16[16,896]{1,0:T(8,128)(2,1)S(1)} %collective-permute-done.5.refs_1_, bf16[16,896]{1,0:T(8,128)(2,1)S(1)} %collective-permute-done.6.refs_2_, ...), custom_call_target="tpu_custom_call" | custom-call | flops 1048576 | bytes 4194304 | tf_op jit(solution)/shard_map/recurrent/pallas_call | solution.py:311
  30.0 2.5 %collective-permute-start.9 = (bf16[16,2048]{1,0:T(8,128)(2,1)S(1)}, bf16[16,2048]{1,0:T(8,128)(2,1)S(1)}, u32[]{:S(2)}, u32[]{:S(2)}) collective-permute-start(bf16[16,2048]{1,0:T(8,128)(2,1)S(1)} %recurrent.1.part_ref), channel_id=1, source_target_pairs={{0,3},{1,2},{2,1},{3,0},{4,7},{5,6},{6,5},{7,4},{8,11},{9,10},{10,... | collective-permute-start | bytes 196616 | tf_op jit(solution)/shard_map/ppermute | solution.py:47
  32.5 0.5 collective-permute-start.8
  33.0 2.3 %collective-permute-done.9.refs_2_ = bf16[16,2048]{1,0:T(8,128)(2,1)S(1)} collective-permute-done((bf16[16,2048]{1,0:T(8,128)(2,1)S(1)}, bf16[16,2048]{1,0:T(8,128)(2,1)S(1)}, u32[]{:S(2)}, u32[]{:S(2)}) %collective-permute-start.9) | collective-permute-done | bytes 65568 | tf_op jit(solution)/shard_map/ppermute | solution.py:47
  35.3 1.6 %collective-permute-start.7 = (bf16[16,2048]{1,0:T(8,128)(2,1)S(1)}, bf16[16,2048]{1,0:T(8,128)(2,1)S(1)}, u32[]{:S(2)}, u32[]{:S(2)}) collective-permute-start(bf16[16,2048]{1,0:T(8,128)(2,1)S(1)} %recurrent.1.part_ref), channel_id=1, source_target_pairs={{0,1},{1,0},{2,3},{3,2},{4,5},{5,4},{6,7},{7,6},{8,9},{9,8},{10,11... | collective-permute-start | bytes 196616 | tf_op jit(solution)/shard_map/ppermute | solution.py:47
  36.9 2.7 %collective-permute-done.7.refs_0_ = bf16[16,2048]{1,0:T(8,128)(2,1)S(1)} collective-permute-done((bf16[16,2048]{1,0:T(8,128)(2,1)S(1)}, bf16[16,2048]{1,0:T(8,128)(2,1)S(1)}, u32[]{:S(2)}, u32[]{:S(2)}) %collective-permute-start.7) | collective-permute-done | bytes 65568 | tf_op jit(solution)/shard_map/ppermute | solution.py:47
  39.9 6.2 %collective-permute-done.12.refs_3_ = bf16[16,2176]{1,0:T(8,128)(2,1)S(1)} collective-permute-done((bf16[16,2176]{1,0:T(8,128)(2,1)S(1)}, bf16[16,2176]{1,0:T(8,128)(2,1)S(1)}, u32[]{:S(2)}, u32[]{:S(2)}) %collective-permute-start.12) | collective-permute-done | bytes 69664 | tf_op jit(solution)/shard_map/ppermute | solution.py:34
  46.2 2.0 %collective-permute-done.11.refs_2_ = bf16[16,2176]{1,0:T(8,128)(2,1)S(1)} collective-permute-done((bf16[16,2176]{1,0:T(8,128)(2,1)S(1)}, bf16[16,2176]{1,0:T(8,128)(2,1)S(1)}, u32[]{:S(2)}, u32[]{:S(2)}) %collective-permute-start.11) | collective-permute-done | bytes 69664 | tf_op jit(solution)/shard_map/ppermute | solution.py:34
  48.2 1.7 %collective-permute-done.10.refs_1_ = bf16[16,2176]{1,0:T(8,128)(2,1)S(1)} collective-permute-done((bf16[16,2176]{1,0:T(8,128)(2,1)S(1)}, bf16[16,2176]{1,0:T(8,128)(2,1)S(1)}, u32[]{:S(2)}, u32[]{:S(2)}) %collective-permute-start.10) | collective-permute-done | bytes 69664 | tf_op jit(solution)/shard_map/ppermute | solution.py:34
  49.9 2.3 %shard_map.177 = (f32[64,512]{1,0:T(8,128)S(1)}, bf16[64,512]{1,0:T(8,128)(2,1)S(1)}, bf16[64,512]{1,0:T(8,128)(2,1)S(1)}, bf16[64,512]{1,0:T(8,128)(2,1)S(1)}) custom-call(bf16[16,2176]{1,0:T(8,128)(2,1)S(1)} %get-tuple-element.51.refs_0_, bf16[16,2176]{1,0:T(8,128)(2,1)S(1)} %collective-permute-done.10.refs_1_, ...), custom_call_target="tpu_custom_call" | custom-call | bytes 13189120 | tf_op jit(solution)/shard_map/pallas_call | solution.py:54
  52.3 1.5 %collective-permute-start.16 = (bf16[64,512]{1,0:T(8,128)(2,1)S(1)}, bf16[64,512]{1,0:T(8,128)(2,1)S(1)}, u32[]{:S(2)}, u32[]{:S(2)}) collective-permute-start(bf16[64,512]{1,0:T(8,128)(2,1)S(1)} %get-tuple-element.56), channel_id=1, source_target_pairs={{0,1},{1,0},{2,3},{3,2},{4,5},{5,4},{6,7},{7,6},{8,9},{9,8},{10,11... | collective-permute-start | bytes 196616 | tf_op jit(solution)/shard_map/ppermute | solution.py:47
  53.8 1.5 %collective-permute-start.17 = (bf16[64,512]{1,0:T(8,128)(2,1)S(1)}, bf16[64,512]{1,0:T(8,128)(2,1)S(1)}, u32[]{:S(2)}, u32[]{:S(2)}) collective-permute-start(bf16[64,512]{1,0:T(8,128)(2,1)S(1)} %get-tuple-element.57), channel_id=1, source_target_pairs={{0,2},{1,3},{2,0},{3,1},{4,6},{5,7},{6,4},{7,5},{8,10},{9,11},{10,... | collective-permute-start | bytes 196616 | tf_op jit(solution)/shard_map/ppermute | solution.py:47
  55.3 0.5 collective-permute-start.18
  55.8 1.1 %collective-permute-done.16 = bf16[64,512]{1,0:T(8,128)(2,1)S(1)} collective-permute-done((bf16[64,512]{1,0:T(8,128)(2,1)S(1)}, bf16[64,512]{1,0:T(8,128)(2,1)S(1)}, u32[]{:S(2)}, u32[]{:S(2)}) %collective-permute-start.16) | collective-permute-done | bytes 65568 | tf_op jit(solution)/shard_map/ppermute | solution.py:47
  56.9 1.8 %collective-permute-done.17 = bf16[64,512]{1,0:T(8,128)(2,1)S(1)} collective-permute-done((bf16[64,512]{1,0:T(8,128)(2,1)S(1)}, bf16[64,512]{1,0:T(8,128)(2,1)S(1)}, u32[]{:S(2)}, u32[]{:S(2)}) %collective-permute-start.17) | collective-permute-done | bytes 65568 | tf_op jit(solution)/shard_map/ppermute | solution.py:47
  58.7 1.8 %collective-permute-done.18 = bf16[64,512]{1,0:T(8,128)(2,1)S(1)} collective-permute-done((bf16[64,512]{1,0:T(8,128)(2,1)S(1)}, bf16[64,512]{1,0:T(8,128)(2,1)S(1)}, u32[]{:S(2)}, u32[]{:S(2)}) %collective-permute-start.18) | collective-permute-done | bytes 65568 | tf_op jit(solution)/shard_map/ppermute | solution.py:47
  60.9 1.6 %collective-permute-start.20 = (bf16[16,512]{1,0:T(8,128)(2,1)S(1)}, bf16[16,512]{1,0:T(8,128)(2,1)S(1)}, u32[]{:S(2)}, u32[]{:S(2)}) collective-permute-start(bf16[16,512]{1,0:T(8,128)(2,1)S(1)} %get-tuple-element.63), channel_id=1, source_target_pairs={{0,20},{4,16},{8,28},{12,24},{16,4},{20,0},{24,12},{28,8},{1,21},{... | collective-permute-start | bytes 49160 | tf_op jit(solution)/shard_map/ppermute | solution.py:34
  62.5 1.2 %collective-permute-done.19 = bf16[16,512]{1,0:T(8,128)(2,1)S(1)} collective-permute-done((bf16[16,512]{1,0:T(8,128)(2,1)S(1)}, bf16[16,512]{1,0:T(8,128)(2,1)S(1)}, u32[]{:S(2)}, u32[]{:S(2)}) %collective-permute-start.19) | collective-permute-done | bytes 16416 | tf_op jit(solution)/shard_map/ppermute | solution.py:34
  63.8 1.9 %collective-permute-done.21 = bf16[16,512]{1,0:T(8,128)(2,1)S(1)} collective-permute-done((bf16[16,512]{1,0:T(8,128)(2,1)S(1)}, bf16[16,512]{1,0:T(8,128)(2,1)S(1)}, u32[]{:S(2)}, u32[]{:S(2)}) %collective-permute-start.21) | collective-permute-done | bytes 16416 | tf_op jit(solution)/shard_map/ppermute | solution.py:34
  65.6 0.6 fusion.3
  (22 shorter events, 2.2 us)
Async XLA Ops:
  2.9 47.0 %collective-permute-start.13 = (bf16[1,2048,512]{2,1,0:T(8,128)(2,1)S(1)}, bf16[1,2048,512]{2,1,0:T(8,128)(2,1)S(1)}, u32[]{:S(2)}, u32[]{:S(2)}) collective-permute-start(bf16[1,2048,512]{2,1,0:T(8,128)(2,1)S(1)} %get-tuple-element.52.refs_4_), channel_id=1, source_target_pairs={{0,4},{4,0},{8,12},{12,8},{16,20},{20,16},{24,28},{28,24},{1,5},{5... | collective-permute-start | bytes 6291464 | tf_op jit(solution)/shard_map/ppermute | solution.py:27
  3.5 46.5 %collective-permute-start.14 = (bf16[1,2048,512]{2,1,0:T(8,128)(2,1)S(1)}, bf16[1,2048,512]{2,1,0:T(8,128)(2,1)S(1)}, u32[]{:S(2)}, u32[]{:S(2)}) collective-permute-start(bf16[1,2048,512]{2,1,0:T(8,128)(2,1)S(1)} %get-tuple-element.53.refs_5_), channel_id=1, source_target_pairs={{0,4},{4,0},{8,12},{12,8},{16,20},{20,16},{24,28},{28,24},{1,5},{5... | collective-permute-start | bytes 6291464 | tf_op jit(solution)/shard_map/ppermute | solution.py:27
  3.5 46.4 %collective-permute-start.15 = (bf16[1,512,2048]{2,1,0:T(8,128)(2,1)S(1)}, bf16[1,512,2048]{2,1,0:T(8,128)(2,1)S(1)}, u32[]{:S(2)}, u32[]{:S(2)}) collective-permute-start(bf16[1,512,2048]{2,1,0:T(8,128)(2,1)S(1)} %get-tuple-element.54.refs_6_), channel_id=1, source_target_pairs={{0,4},{4,0},{8,12},{12,8},{16,20},{20,16},{24,28},{28,24},{1,5},{5... | collective-permute-start | bytes 6291464 | tf_op jit(solution)/shard_map/ppermute | solution.py:27
  5.2 15.1 %collective-permute-start.3 = (bf16[256,896]{1,0:T(8,128)(2,1)S(1)}, bf16[256,896]{1,0:T(8,128)(2,1)S(1)}, u32[]{:S(2)}, u32[]{:S(2)}) collective-permute-start(bf16[256,896]{1,0:T(8,128)(2,1)S(1)} %get-tuple-element.38.refs_4_), channel_id=1, source_target_pairs={{0,4},{4,0},{8,12},{12,8},{16,20},{20,16},{24,28},{28,24},{1,5},{5... | collective-permute-start | bytes 1376264 | tf_op jit(solution)/shard_map/ppermute | solution.py:27
  5.4 4.1 %collective-permute-start = (bf16[16,512]{1,0:T(8,128)(2,1)S(1)}, bf16[16,512]{1,0:T(8,128)(2,1)S(1)}, u32[]{:S(2)}, u32[]{:S(2)}) collective-permute-start(bf16[16,512]{1,0:T(8,128)(2,1)S(1)} %get-tuple-element.35), channel_id=1, source_target_pairs={{0,12},{4,8},{8,4},{12,0},{16,28},{20,24},{24,20},{28,16},{1,13},{... | collective-permute-start | bytes 49160 | tf_op jit(solution)/shard_map/ppermute | solution.py:34
  9.5 4.2 %collective-permute-start.1 = (bf16[16,512]{1,0:T(8,128)(2,1)S(1)}, bf16[16,512]{1,0:T(8,128)(2,1)S(1)}, u32[]{:S(2)}, u32[]{:S(2)}) collective-permute-start(bf16[16,512]{1,0:T(8,128)(2,1)S(1)} %get-tuple-element.36), channel_id=1, source_target_pairs={{0,20},{4,16},{8,28},{12,24},{16,4},{20,0},{24,12},{28,8},{1,21},{... | collective-permute-start | bytes 49160 | tf_op jit(solution)/shard_map/ppermute | solution.py:34
  13.7 6.6 %collective-permute-start.2 = (bf16[16,512]{1,0:T(8,128)(2,1)S(1)}, bf16[16,512]{1,0:T(8,128)(2,1)S(1)}, u32[]{:S(2)}, u32[]{:S(2)}) collective-permute-start(bf16[16,512]{1,0:T(8,128)(2,1)S(1)} %get-tuple-element.37), channel_id=1, source_target_pairs={{0,28},{4,24},{8,20},{12,16},{16,12},{20,8},{24,4},{28,0},{1,29},{... | collective-permute-start | bytes 49160 | tf_op jit(solution)/shard_map/ppermute | solution.py:34
  20.6 3.4 %collective-permute-start.4 = (bf16[16,896]{1,0:T(8,128)(2,1)S(1)}, bf16[16,896]{1,0:T(8,128)(2,1)S(1)}, u32[]{:S(2)}, u32[]{:S(2)}) collective-permute-start(bf16[16,896]{1,0:T(8,128)(2,1)S(1)} %get-tuple-element.40), channel_id=1, source_target_pairs={{0,12},{4,8},{8,4},{12,0},{16,28},{20,24},{24,20},{28,16},{1,13},{... | collective-permute-start | bytes 86024 | tf_op jit(solution)/shard_map/ppermute | solution.py:34
  20.7 5.6 %collective-permute-start.5 = (bf16[16,896]{1,0:T(8,128)(2,1)S(1)}, bf16[16,896]{1,0:T(8,128)(2,1)S(1)}, u32[]{:S(2)}, u32[]{:S(2)}) collective-permute-start(bf16[16,896]{1,0:T(8,128)(2,1)S(1)} %get-tuple-element.41), channel_id=1, source_target_pairs={{0,20},{4,16},{8,28},{12,24},{16,4},{20,0},{24,12},{28,8},{1,21},{... | collective-permute-start | bytes 86024 | tf_op jit(solution)/shard_map/ppermute | solution.py:34
  24.0 5.1 %collective-permute-start.6 = (bf16[16,896]{1,0:T(8,128)(2,1)S(1)}, bf16[16,896]{1,0:T(8,128)(2,1)S(1)}, u32[]{:S(2)}, u32[]{:S(2)}) collective-permute-start(bf16[16,896]{1,0:T(8,128)(2,1)S(1)} %get-tuple-element.42), channel_id=1, source_target_pairs={{0,28},{4,24},{8,20},{12,16},{16,12},{20,8},{24,4},{28,0},{1,29},{... | collective-permute-start | bytes 86024 | tf_op jit(solution)/shard_map/ppermute | solution.py:34
  30.0 5.3 %collective-permute-start.9 = (bf16[16,2048]{1,0:T(8,128)(2,1)S(1)}, bf16[16,2048]{1,0:T(8,128)(2,1)S(1)}, u32[]{:S(2)}, u32[]{:S(2)}) collective-permute-start(bf16[16,2048]{1,0:T(8,128)(2,1)S(1)} %recurrent.1.part_ref), channel_id=1, source_target_pairs={{0,3},{1,2},{2,1},{3,0},{4,7},{5,6},{6,5},{7,4},{8,11},{9,10},{10,... | collective-permute-start | bytes 196616 | tf_op jit(solution)/shard_map/ppermute | solution.py:47
  32.5 4.4 %collective-permute-start.8 = (bf16[16,2048]{1,0:T(8,128)(2,1)S(1)}, bf16[16,2048]{1,0:T(8,128)(2,1)S(1)}, u32[]{:S(2)}, u32[]{:S(2)}) collective-permute-start(bf16[16,2048]{1,0:T(8,128)(2,1)S(1)} %recurrent.1.part_ref), channel_id=1, source_target_pairs={{0,2},{1,3},{2,0},{3,1},{4,6},{5,7},{6,4},{7,5},{8,10},{9,11},{10,... | collective-permute-start | bytes 196616 | tf_op jit(solution)/shard_map/ppermute | solution.py:47
  35.3 4.3 %collective-permute-start.7 = (bf16[16,2048]{1,0:T(8,128)(2,1)S(1)}, bf16[16,2048]{1,0:T(8,128)(2,1)S(1)}, u32[]{:S(2)}, u32[]{:S(2)}) collective-permute-start(bf16[16,2048]{1,0:T(8,128)(2,1)S(1)} %recurrent.1.part_ref), channel_id=1, source_target_pairs={{0,1},{1,0},{2,3},{3,2},{4,5},{5,4},{6,7},{7,6},{8,9},{9,8},{10,11... | collective-permute-start | bytes 196616 | tf_op jit(solution)/shard_map/ppermute | solution.py:47
  39.8 6.4 %collective-permute-start.12 = (bf16[16,2176]{1,0:T(8,128)(2,1)S(1)}, bf16[16,2176]{1,0:T(8,128)(2,1)S(1)}, u32[]{:S(2)}, u32[]{:S(2)}) collective-permute-start(bf16[16,2176]{1,0:T(8,128)(2,1)S(1)} %get-tuple-element.51.refs_0_), channel_id=1, source_target_pairs={{0,28},{4,24},{8,20},{12,16},{16,12},{20,8},{24,4},{28,0},{1,29},{... | collective-permute-start | bytes 208904 | tf_op jit(solution)/shard_map/ppermute | solution.py:34
  39.9 8.4 %collective-permute-start.11 = (bf16[16,2176]{1,0:T(8,128)(2,1)S(1)}, bf16[16,2176]{1,0:T(8,128)(2,1)S(1)}, u32[]{:S(2)}, u32[]{:S(2)}) collective-permute-start(bf16[16,2176]{1,0:T(8,128)(2,1)S(1)} %get-tuple-element.51.refs_0_), channel_id=1, source_target_pairs={{0,20},{4,16},{8,28},{12,24},{16,4},{20,0},{24,12},{28,8},{1,21},{... | collective-permute-start | bytes 208904 | tf_op jit(solution)/shard_map/ppermute | solution.py:34
  46.2 3.7 %collective-permute-start.10 = (bf16[16,2176]{1,0:T(8,128)(2,1)S(1)}, bf16[16,2176]{1,0:T(8,128)(2,1)S(1)}, u32[]{:S(2)}, u32[]{:S(2)}) collective-permute-start(bf16[16,2176]{1,0:T(8,128)(2,1)S(1)} %get-tuple-element.51.refs_0_), channel_id=1, source_target_pairs={{0,12},{4,8},{8,4},{12,0},{16,28},{20,24},{24,20},{28,16},{1,13},{... | collective-permute-start | bytes 208904 | tf_op jit(solution)/shard_map/ppermute | solution.py:34
  52.3 4.7 %collective-permute-start.16 = (bf16[64,512]{1,0:T(8,128)(2,1)S(1)}, bf16[64,512]{1,0:T(8,128)(2,1)S(1)}, u32[]{:S(2)}, u32[]{:S(2)}) collective-permute-start(bf16[64,512]{1,0:T(8,128)(2,1)S(1)} %get-tuple-element.56), channel_id=1, source_target_pairs={{0,1},{1,0},{2,3},{3,2},{4,5},{5,4},{6,7},{7,6},{8,9},{9,8},{10,11... | collective-permute-start | bytes 196616 | tf_op jit(solution)/shard_map/ppermute | solution.py:47
  53.8 4.9 %collective-permute-start.17 = (bf16[64,512]{1,0:T(8,128)(2,1)S(1)}, bf16[64,512]{1,0:T(8,128)(2,1)S(1)}, u32[]{:S(2)}, u32[]{:S(2)}) collective-permute-start(bf16[64,512]{1,0:T(8,128)(2,1)S(1)} %get-tuple-element.57), channel_id=1, source_target_pairs={{0,2},{1,3},{2,0},{3,1},{4,6},{5,7},{6,4},{7,5},{8,10},{9,11},{10,... | collective-permute-start | bytes 196616 | tf_op jit(solution)/shard_map/ppermute | solution.py:47
  55.3 5.2 %collective-permute-start.18 = (bf16[64,512]{1,0:T(8,128)(2,1)S(1)}, bf16[64,512]{1,0:T(8,128)(2,1)S(1)}, u32[]{:S(2)}, u32[]{:S(2)}) collective-permute-start(bf16[64,512]{1,0:T(8,128)(2,1)S(1)} %get-tuple-element.58), channel_id=1, source_target_pairs={{0,3},{1,2},{2,1},{3,0},{4,7},{5,6},{6,5},{7,4},{8,11},{9,10},{10,... | collective-permute-start | bytes 196616 | tf_op jit(solution)/shard_map/ppermute | solution.py:47
  60.5 3.2 %collective-permute-start.19 = (bf16[16,512]{1,0:T(8,128)(2,1)S(1)}, bf16[16,512]{1,0:T(8,128)(2,1)S(1)}, u32[]{:S(2)}, u32[]{:S(2)}) collective-permute-start(bf16[16,512]{1,0:T(8,128)(2,1)S(1)} %get-tuple-element.61), channel_id=1, source_target_pairs={{0,12},{4,8},{8,4},{12,0},{16,28},{20,24},{24,20},{28,16},{1,13},{... | collective-permute-start | bytes 49160 | tf_op jit(solution)/shard_map/ppermute | solution.py:34
  60.6 5.0 %collective-permute-start.21 = (bf16[16,512]{1,0:T(8,128)(2,1)S(1)}, bf16[16,512]{1,0:T(8,128)(2,1)S(1)}, u32[]{:S(2)}, u32[]{:S(2)}) collective-permute-start(bf16[16,512]{1,0:T(8,128)(2,1)S(1)} %get-tuple-element.62), channel_id=1, source_target_pairs={{0,28},{4,24},{8,20},{12,16},{16,12},{20,8},{24,4},{28,0},{1,29},{... | collective-permute-start | bytes 49160 | tf_op jit(solution)/shard_map/ppermute | solution.py:34
  60.9 4.7 %collective-permute-start.20 = (bf16[16,512]{1,0:T(8,128)(2,1)S(1)}, bf16[16,512]{1,0:T(8,128)(2,1)S(1)}, u32[]{:S(2)}, u32[]{:S(2)}) collective-permute-start(bf16[16,512]{1,0:T(8,128)(2,1)S(1)} %get-tuple-element.63), channel_id=1, source_target_pairs={{0,20},{4,16},{8,28},{12,24},{16,4},{20,0},{24,12},{28,8},{1,21},{... | collective-permute-start | bytes 49160 | tf_op jit(solution)/shard_map/ppermute | solution.py:34

commit v2 on v1

--- a/solution.py
+++ b/solution.py
@@ -90,9 +90,8 @@
         copy.wait()
 
 
-def spread_kernel(weights, *refs):
-    tokens_ref, weight_refs, refs = refs[0], refs[1 : 1 + weights], refs[1 + weights :]
-    *block_refs, near_ref, joined_ref, sems = refs
+def spread_kernel(tokens_ref, *refs):
+    *block_refs, near_ref, sems = refs
     chip = lax.axis_index("ep") // 2
     cols = block_refs[0].shape[1]
     pairs = []
@@ -100,7 +99,13 @@
         at = pl.ds(pl.multiple_of((chip ^ k) * cols, lane_tile), cols)
         pairs.append((tokens_ref.at[:, at], block_refs[k]))
     pairs.append((tokens_ref, near_ref))
-    at = 0
+    for copy in load(pairs, sems):
+        copy.wait()
+
+
+def join_kernel(*refs):
+    *weight_refs, joined_ref, sems = refs
+    pairs, at = [], 0
     for weight in weight_refs:
         pairs.append((weight, joined_ref.at[:, at : at + weight.shape[1]]))
         at += weight.shape[1]
@@ -210,23 +215,37 @@
     me, experts = lax.axis_index("ep"), lax.axis_size("ep")
     head = lax.axis_index("tp")
     place = lax.broadcasted_iota(jnp.int32, share.shape, 1)
+    *pieces, first_hidden, second_hidden, factor_ref = outs
     hiddens, factors = [], []
-    for n in range(2):
+    for n, hidden_ref in enumerate((first_hidden, second_hidden)):
         gate_ref, up_ref = weights[3 * n], weights[3 * n + 1]
         chosen = (place == me ^ n) | (place == (me ^ n) + experts)
         factors.append(jnp.sum(jnp.where(chosen, share, 0.0), axis=1, keepdims=True))
         gate = jnp.dot(rows, gate_ref[0], preferred_element_type=wide)
         upper = jnp.dot(rows, up_ref[0], preferred_element_type=wide)
         hiddens.append((silu(gate) * upper).astype(narrow))
-    cols = outs[0].shape[1]
-    for k, out in enumerate(outs):
-        at = pl.ds(pl.multiple_of((head ^ k) * cols, lane_tile), cols)
-        total = None
-        for n in range(2):
-            down_ref = weights[3 * n + 2]
-            part = jnp.dot(hiddens[n], down_ref[0, :, at], preferred_element_type=wide) * factors[n]
-            total = part if total is None else total + part
-        out[...] = total.astype(out.dtype)
+        hidden_ref[...] = hiddens[n]
+        factor_ref[:, n : n + 1] = factors[n]
+    cols = pieces[0].shape[1]
+    for k, out in enumerate(pieces):
+        at = pl.ds(pl.multiple_of((head ^ (k + 1)) * cols, lane_tile), cols)
+        out[...] = weighted(hiddens, factors, (weights[2], weights[5]), at).astype(out.dtype)
+
+
+def weighted(hiddens, factors, downs, at):
+    parts = [
+        jnp.dot(hidden, down[0, :, at], preferred_element_type=wide) * factor
+        for hidden, factor, down in zip(hiddens, factors, downs)
+    ]
+    return parts[0] + parts[1]
+
+
+def near_kernel(first_ref, second_ref, factor_ref, down_ref, other_down_ref, out_ref):
+    cols = out_ref.shape[1]
+    at = pl.ds(pl.multiple_of(lax.axis_index("tp") * cols, lane_tile), cols)
+    factors = factor_ref[:, 0:1], factor_ref[:, 1:2]
+    hiddens = first_ref[...], second_ref[...]
+    out_ref[...] = weighted(hiddens, factors, (down_ref, other_down_ref), at)
 
 
 def on_device(
@@ -262,13 +281,13 @@
     mib = 1 << 20
 
     weights = (w_query, w_key, w_decay, w_value, w_outgate)
-    *pair_cols, tokens_near, joined = load_call(
-        functools.partial(spread_kernel, len(weights)),
-        (tokens, *weights),
-        [like((seqs, 2 * feats), narrow)] * chips
-        + [like(tokens.shape, narrow), like((feats, proj_cols), narrow)],
-        chips + 1 + len(weights),
-    )
+    *pair_cols, tokens_near = load_call(
+        spread_kernel,
+        (tokens,),
+        [like((seqs, 2 * feats), narrow)] * chips + [like(tokens.shape, narrow)],
+        chips + 1,
+    )
+    (joined,) = load_call(join_kernel, weights, [like((feats, proj_cols), narrow)], len(weights))
     blocks = [pair_cols[0], *swap_chips(pair_cols)]
     joined_other = swap_core(joined)
     side_args = (
@@ -279,8 +298,6 @@
         decay_rate[None, :],
         head_gain[None, :],
         moe_gain[None, :],
-        w_output,
-        state,
     )
     loaded = load_call(
         functools.partial(side_kernel, len(side_args)),
@@ -290,7 +307,7 @@
         len(side_args),
         near=(tokens_near,),
     )
-    gain, rate, read_gain, mix_gain, output_near, state_near, scale, share = loaded[3:]
+    gain, rate, read_gain, mix_gain, scale, share = loaded[3:]
     base, *sums = call(
         functools.partial(project_kernel, chips),
         [like((seqs, proj_cols), wide)] + [like((seqs, proj_cols), narrow)] * (chips - 1),
@@ -298,14 +315,13 @@
         8 * mib,
     )
     arrived = swap_chips([base, *sums])
-    expert_weights = (w_gate, w_up, w_down)
-    expert_weights = load_call(
-        functools.partial(load_kernel, 3),
-        expert_weights,
-        [like(a.shape, a.dtype) for a in expert_weights],
-        3,
-    )
-    other_weights = []
+    output_near, state_near = load_call(
+        functools.partial(load_kernel, 2),
+        (w_output, state),
+        [like(a.shape, a.dtype) for a in (w_output, state)],
+        2,
+    )
+    expert_weights, other_weights = (w_gate, w_up, w_down), []
     for weight in expert_weights:
         other_weights.append(swap_core(weight))
     (part,) = pl.pallas_call(
@@ -326,13 +342,29 @@
         4 * mib,
     )
     rows = [sending, *swap_chips([sending] * chips)]
-    head_sum, *pieces = call(
+    expert_weights = load_call(
+        functools.partial(load_kernel, 3),
+        expert_weights,
+        [like(a.shape, a.dtype) for a in expert_weights],
+        3,
+    )
+    hidden_cols = w_gate.shape[2]
+    *pieces, first_hidden, second_hidden, factor = call(
         functools.partial(expert_kernel, chips),
-        [like((half, cols), wide)] + [like((half, cols), narrow)] * (tp_count - 1),
+        [like((half, cols), narrow)] * (tp_count - 1)
+        + [like((half, hidden_cols), narrow)] * 2
+        + [like((half, lane_tile), wide)],
         (*rows, *expert_weights, *other_weights),
         24 * mib,
     )
-    for block in swap_heads([head_sum, *pieces], 0):
+    arrived = swap_heads([None, *pieces], 0)
+    (head_sum,) = call(
+        near_kernel,
+        [like((half, cols), wide)],
+        (first_hidden, second_hidden, factor, expert_weights[2], other_weights[2]),
+        16 * mib,
+    )
+    for block in arrived:
         head_sum = head_sum + block.astype(wide)
     head_narrow = head_sum.astype(narrow)
     moe_sum = head_sum[:seqs]

time: 66.9 us -> 64.8 us (0.969)
  waiting for transfers between devices: 29 us -> 23.1 us
  starting transfers between devices: 26 us -> 28 us
  Pallas kernels: 10.5 us -> 12.2 us
    ppermute x12, waiting for transfers between devices: 19.2 us -> 13.7 us  [swap_chips(): lax.ppermute(blocks[k], 'ep', [(i, i ^ 2 * k + 1) for i in range(count)])]
    ppermute x12, starting transfers between devices: 16.7 us -> 18.9 us  [swap_chips(): lax.ppermute(blocks[k], 'ep', [(i, i ^ 2 * k + 1) for i in range(count)])]
    pallas_call x3 -> x5, Pallas kernels: 6.81 us -> 8.38 us  [load_call(): pl.pallas_call(kernel, out_shape=tuple(outs), in_specs=[pl.BlockSpec(memo...]
    pallas_call x3 -> x4, Pallas kernels: 2.76 us -> 2.88 us  [call(): pl.pallas_call(kernel, out_shape=tuple(outs), in_specs=[pl.BlockSpec(memo...]
  transfers between devices with their start and end apart: 22 -> 22, of which waited for: 14 -> 13; matrix products, arithmetic and copies ran while one was open for 0% -> 0% of each run, Pallas kernels for 8% -> 16%
where the time goes in v2:
time: 64.8 us; the launch traced here: 64.1 us
  starting transfers between devices  28 us (43%)
  waiting for transfers between devices  23.1 us (36%)
  Pallas kernels  12.2 us (19%)
  other arithmetic  0.66 us (1%)
    ppermute x12, starting transfers between devices, swap_chips(): lax.ppermute(blocks[k], 'ep', [(i, i ^ 2 * k + 1) for i in range(count)])  18.9 us
    ppermute x12, waiting for transfers between devices, swap_chips(): lax.ppermute(blocks[k], 'ep', [(i, i ^ 2 * k + 1) for i in range(count)])  13.7 us
    ppermute x6, waiting for transfers between devices, swap_heads(): got[k] = lax.ppermute(blocks[k], ('ep', 'tp'), pairs)  9.39 us
    pallas_call x5, Pallas kernels, load_call(): pl.pallas_call(kernel, out_shape=tuple(outs), in_specs=[pl.BlockSpec(memo...  8.38 us
    ppermute x6, starting transfers between devices, swap_heads(): got[k] = lax.ppermute(blocks[k], ('ep', 'tp'), pairs)  8 us
    pallas_call x4, Pallas kernels, call(): pl.pallas_call(kernel, out_shape=tuple(outs), in_specs=[pl.BlockSpec(memo...  2.88 us
  transfers between devices with their start and end apart: 22, of which 13 were waited for; matrix products, arithmetic and copies ran while one was open for 0% of the time, Pallas kernels for 16%

profile of v2, /device:TPU:0, one launch (start us, length us, event | category | flops | bytes accessed | tf_op | source)
XLA Modules:
  0.0 64.1 jit_solution(12694302465606487247)
XLA Ops:
  0.0 0.5 collective-permute-start.13
  0.5 0.5 collective-permute-start.15
  1.0 1.1 %shard_map.174.refs_4_ = bf16[256,896]{1,0:T(8,128)(2,1)S(1)} custom-call(bf16[256,128]{1,0:T(8,128)(2,1)} %refs_0_.3, bf16[256,128]{1,0:T(8,128)(2,1)} %refs_1_.3, bf16[256,128]{1,0:T(8,128)(2,1)} %refs_2_.2, bf16[256,256]{1,0:T(8,128)(2,1)} %refs_3_.1, bf16[256,256]{1,0:T(8,128)(2,1)} %refs_4_.1), custom_call_target="tpu_custom_call" | custom-call | flops 4194304 | bytes 4194304 | tf_op jit(solution)/shard_map/pallas_call | solution.py:65
  2.2 1.0 %shard_map.172 = (bf16[16,512]{1,0:T(8,128)(2,1)S(1)}, bf16[16,512]{1,0:T(8,128)(2,1)S(1)}, bf16[16,512]{1,0:T(8,128)(2,1)S(1)}, bf16[16,512]{1,0:T(8,128)(2,1)S(1)}, bf16[16,2048]{1,0:T(8,128)(2,1)S(1)}) custom-call(bf16[16,2048]{1,0:T(8,128)(2,1)} %tokens_ref.1), custom_call_target="tpu_custom_call" | custom-call | flops 4194304 | bytes 4194304 | tf_op jit(solution)/shard_map/pallas_call | solution.py:65
  3.2 2.7 %collective-permute-start = (bf16[16,512]{1,0:T(8,128)(2,1)S(1)}, bf16[16,512]{1,0:T(8,128)(2,1)S(1)}, u32[]{:S(2)}, u32[]{:S(2)}) collective-permute-start(bf16[16,512]{1,0:T(8,128)(2,1)S(1)} %get-tuple-element.36), channel_id=1, source_target_pairs={{0,12},{4,8},{8,4},{12,0},{16,28},{20,24},{24,20},{28,16},{1,13},{... | collective-permute-start | bytes 49160 | tf_op jit(solution)/shard_map/ppermute | solution.py:34
  5.9 1.4 %collective-permute-done.refs_1_ = bf16[16,512]{1,0:T(8,128)(2,1)S(1)} collective-permute-done((bf16[16,512]{1,0:T(8,128)(2,1)S(1)}, bf16[16,512]{1,0:T(8,128)(2,1)S(1)}, u32[]{:S(2)}, u32[]{:S(2)}) %collective-permute-start) | collective-permute-done | bytes 16416 | tf_op jit(solution)/shard_map/ppermute | solution.py:34
  7.4 2.8 %collective-permute-start.1 = (bf16[16,512]{1,0:T(8,128)(2,1)S(1)}, bf16[16,512]{1,0:T(8,128)(2,1)S(1)}, u32[]{:S(2)}, u32[]{:S(2)}) collective-permute-start(bf16[16,512]{1,0:T(8,128)(2,1)S(1)} %get-tuple-element.37), channel_id=1, source_target_pairs={{0,20},{4,16},{8,28},{12,24},{16,4},{20,0},{24,12},{28,8},{1,21},{... | collective-permute-start | bytes 49160 | tf_op jit(solution)/shard_map/ppermute | solution.py:34
  10.2 1.4 %collective-permute-done.1.refs_2_ = bf16[16,512]{1,0:T(8,128)(2,1)S(1)} collective-permute-done((bf16[16,512]{1,0:T(8,128)(2,1)S(1)}, bf16[16,512]{1,0:T(8,128)(2,1)S(1)}, u32[]{:S(2)}, u32[]{:S(2)}) %collective-permute-start.1) | collective-permute-done | bytes 16416 | tf_op jit(solution)/shard_map/ppermute | solution.py:34
  11.6 3.9 %collective-permute-start.2 = (bf16[16,512]{1,0:T(8,128)(2,1)S(1)}, bf16[16,512]{1,0:T(8,128)(2,1)S(1)}, u32[]{:S(2)}, u32[]{:S(2)}) collective-permute-start(bf16[16,512]{1,0:T(8,128)(2,1)S(1)} %get-tuple-element.38), channel_id=1, source_target_pairs={{0,28},{4,24},{8,20},{12,16},{16,12},{20,8},{24,4},{28,0},{1,29},{... | collective-permute-start | bytes 49160 | tf_op jit(solution)/shard_map/ppermute | solution.py:34
  15.6 1.5 %shard_map.173 = (s32[2,16]{1,0:T(2,128)}, f32[1,16]{1,0:T(1,128)}, f32[2,16]{1,0:T(2,128)}, f32[1,2048]{1,0:T(1,128)S(1)}, f32[1,128]{1,0:T(1,128)S(1)}, /*inde...) custom-call(bf16[16,2048]{1,0:T(8,128)(2,1)S(1)} %get-tuple-element.33.refs_0_.toke, ...), custom_call_target="tpu_custom_call" | custom-call | flops 4194304 | bytes 4194304 | tf_op jit(solution)/shard_map/pallas_call | solution.py:65
  17.4 4.0 %collective-permute-start.5 = (bf16[16,896]{1,0:T(8,128)(2,1)S(1)}, bf16[16,896]{1,0:T(8,128)(2,1)S(1)}, u32[]{:S(2)}, u32[]{:S(2)}) collective-permute-start(bf16[16,896]{1,0:T(8,128)(2,1)S(1)} %get-tuple-element.41), channel_id=1, source_target_pairs={{0,20},{4,16},{8,28},{12,24},{16,4},{20,0},{24,12},{28,8},{1,21},{... | collective-permute-start | bytes 86024 | tf_op jit(solution)/shard_map/ppermute | solution.py:34
  21.4 2.7 %collective-permute-start.6 = (bf16[16,896]{1,0:T(8,128)(2,1)S(1)}, bf16[16,896]{1,0:T(8,128)(2,1)S(1)}, u32[]{:S(2)}, u32[]{:S(2)}) collective-permute-start(bf16[16,896]{1,0:T(8,128)(2,1)S(1)} %get-tuple-element.42), channel_id=1, source_target_pairs={{0,28},{4,24},{8,20},{12,16},{16,12},{20,8},{24,4},{28,0},{1,29},{... | collective-permute-start | bytes 86024 | tf_op jit(solution)/shard_map/ppermute | solution.py:34
  24.2 1.9 %shard_map.176 = (bf16[256,2048]{1,0:T(8,128)(2,1)S(1)}, f32[16,1,128,256]{3,2,1,0:T(8,128)S(1)}) custom-call(bf16[256,2048]{1,0:T(8,128)(2,1)} %refs_0_.4, f32[16,1,128,256]{3,2,1,0:T(8,128)} %refs_1_.4), custom_call_target="tpu_custom_call" | custom-call | flops 4194304 | bytes 4194304 | tf_op jit(solution)/shard_map/pallas_call | solution.py:65
  26.6 1.0 %recurrent.1.part_ref = bf16[16,2048]{1,0:T(8,128)(2,1)S(1)} custom-call(f32[16,896]{1,0:T(8,128)S(1)} %get-tuple-element.39.base_ref, bf16[16,896]{1,0:T(8,128)(2,1)S(1)} %collective-permute-done.4.refs_0_, bf16[16,896]{1,0:T(8,128)(2,1)S(1)} %collective-permute-done.5.refs_1_, bf16[16,896]{1,0:T(8,128)(2,1)S(1)} %collective-permute-done.6.refs_2_, ...), custom_call_target="tpu_custom_call" | custom-call | flops 1048576 | bytes 4194304 | tf_op jit(solution)/shard_map/recurrent/pallas_call | solution.py:327
  27.5 2.5 %collective-permute-start.9 = (bf16[16,2048]{1,0:T(8,128)(2,1)S(1)}, bf16[16,2048]{1,0:T(8,128)(2,1)S(1)}, u32[]{:S(2)}, u32[]{:S(2)}) collective-permute-start(bf16[16,2048]{1,0:T(8,128)(2,1)S(1)} %recurrent.1.part_ref), channel_id=1, source_target_pairs={{0,3},{1,2},{2,1},{3,0},{4,7},{5,6},{6,5},{7,4},{8,11},{9,10},{10,... | collective-permute-start | bytes 196616 | tf_op jit(solution)/shard_map/ppermute | solution.py:47
  30.0 0.5 collective-permute-start.8
  30.5 2.2 %collective-permute-done.9.refs_2_ = bf16[16,2048]{1,0:T(8,128)(2,1)S(1)} collective-permute-done((bf16[16,2048]{1,0:T(8,128)(2,1)S(1)}, bf16[16,2048]{1,0:T(8,128)(2,1)S(1)}, u32[]{:S(2)}, u32[]{:S(2)}) %collective-permute-start.9) | collective-permute-done | bytes 65568 | tf_op jit(solution)/shard_map/ppermute | solution.py:47
  32.7 1.5 %collective-permute-start.7 = (bf16[16,2048]{1,0:T(8,128)(2,1)S(1)}, bf16[16,2048]{1,0:T(8,128)(2,1)S(1)}, u32[]{:S(2)}, u32[]{:S(2)}) collective-permute-start(bf16[16,2048]{1,0:T(8,128)(2,1)S(1)} %recurrent.1.part_ref), channel_id=1, source_target_pairs={{0,1},{1,0},{2,3},{3,2},{4,5},{5,4},{6,7},{7,6},{8,9},{9,8},{10,11... | collective-permute-start | bytes 196616 | tf_op jit(solution)/shard_map/ppermute | solution.py:47
  34.3 2.7 %collective-permute-done.7.refs_0_ = bf16[16,2048]{1,0:T(8,128)(2,1)S(1)} collective-permute-done((bf16[16,2048]{1,0:T(8,128)(2,1)S(1)}, bf16[16,2048]{1,0:T(8,128)(2,1)S(1)}, u32[]{:S(2)}, u32[]{:S(2)}) %collective-permute-start.7) | collective-permute-done | bytes 65568 | tf_op jit(solution)/shard_map/ppermute | solution.py:47
  37.7 5.9 %collective-permute-done.12.refs_3_ = bf16[16,2176]{1,0:T(8,128)(2,1)S(1)} collective-permute-done((bf16[16,2176]{1,0:T(8,128)(2,1)S(1)}, bf16[16,2176]{1,0:T(8,128)(2,1)S(1)}, u32[]{:S(2)}, u32[]{:S(2)}) %collective-permute-start.12) | collective-permute-done | bytes 69664 | tf_op jit(solution)/shard_map/ppermute | solution.py:34
  43.6 2.9 %shard_map.178 = (bf16[1,2048,512]{2,1,0:T(8,128)(2,1)S(1)}, bf16[1,2048,512]{2,1,0:T(8,128)(2,1)S(1)}, bf16[1,512,2048]{2,1,0:T(8,128)(2,1)S(1)}) custom-call(bf16[1,2048,512]{2,1,0:T(8,128)(2,1)} %refs_0_.5, bf16[1,2048,512]{2,1,0:T(8,128)(2,1)} %refs_1_.5, bf16[1,512,2048]{2,1,0:T(8,128)(2,1)} %refs_2_.3), custom_call_target="tpu_custom_call" | custom-call | flops 4194304 | bytes 4194304 | tf_op jit(solution)/shard_map/pallas_call | solution.py:65
  46.5 1.4 %collective-permute-done.10.refs_1_ = bf16[16,2176]{1,0:T(8,128)(2,1)S(1)} collective-permute-done((bf16[16,2176]{1,0:T(8,128)(2,1)S(1)}, bf16[16,2176]{1,0:T(8,128)(2,1)S(1)}, u32[]{:S(2)}, u32[]{:S(2)}) %collective-permute-start.10) | collective-permute-done | bytes 69664 | tf_op jit(solution)/shard_map/ppermute | solution.py:34
  47.9 2.1 %shard_map.179 = (bf16[64,512]{1,0:T(8,128)(2,1)S(1)}, bf16[64,512]{1,0:T(8,128)(2,1)S(1)}, bf16[64,512]{1,0:T(8,128)(2,1)S(1)}, bf16[64,512]{1,0:T(8,128)(2,1)S...) custom-call(bf16[16,2176]{1,0:T(8,128)(2,1)S(1)} %get-tuple-element.51.refs_0_, ...), custom_call_target="tpu_custom_call" | custom-call | bytes 13221888 | tf_op jit(solution)/shard_map/pallas_call | solution.py:54
  50.0 1.5 %collective-permute-start.16 = (bf16[64,512]{1,0:T(8,128)(2,1)S(1)}, bf16[64,512]{1,0:T(8,128)(2,1)S(1)}, u32[]{:S(2)}, u32[]{:S(2)}) collective-permute-start(bf16[64,512]{1,0:T(8,128)(2,1)S(1)} %get-tuple-element.58), channel_id=1, source_target_pairs={{0,1},{1,0},{2,3},{3,2},{4,5},{5,4},{6,7},{7,6},{8,9},{9,8},{10,11... | collective-permute-start | bytes 196616 | tf_op jit(solution)/shard_map/ppermute | solution.py:47
  51.6 1.5 %collective-permute-start.17 = (bf16[64,512]{1,0:T(8,128)(2,1)S(1)}, bf16[64,512]{1,0:T(8,128)(2,1)S(1)}, u32[]{:S(2)}, u32[]{:S(2)}) collective-permute-start(bf16[64,512]{1,0:T(8,128)(2,1)S(1)} %get-tuple-element.59), channel_id=1, source_target_pairs={{0,2},{1,3},{2,0},{3,1},{4,6},{5,7},{6,4},{7,5},{8,10},{9,11},{10,... | collective-permute-start | bytes 196616 | tf_op jit(solution)/shard_map/ppermute | solution.py:47
  53.1 0.5 collective-permute-start.18
  54.4 1.5 %collective-permute-done.17 = bf16[64,512]{1,0:T(8,128)(2,1)S(1)} collective-permute-done((bf16[64,512]{1,0:T(8,128)(2,1)S(1)}, bf16[64,512]{1,0:T(8,128)(2,1)S(1)}, u32[]{:S(2)}, u32[]{:S(2)}) %collective-permute-start.17) | collective-permute-done | bytes 65568 | tf_op jit(solution)/shard_map/ppermute | solution.py:47
  55.8 2.4 %collective-permute-done.18 = bf16[64,512]{1,0:T(8,128)(2,1)S(1)} collective-permute-done((bf16[64,512]{1,0:T(8,128)(2,1)S(1)}, bf16[64,512]{1,0:T(8,128)(2,1)S(1)}, u32[]{:S(2)}, u32[]{:S(2)}) %collective-permute-start.18) | collective-permute-done | bytes 65568 | tf_op jit(solution)/shard_map/ppermute | solution.py:47
  58.5 1.9 %collective-permute-start.20 = (bf16[16,512]{1,0:T(8,128)(2,1)S(1)}, bf16[16,512]{1,0:T(8,128)(2,1)S(1)}, u32[]{:S(2)}, u32[]{:S(2)}) collective-permute-start(bf16[16,512]{1,0:T(8,128)(2,1)S(1)} %get-tuple-element.65), channel_id=1, source_target_pairs={{0,20},{4,16},{8,28},{12,24},{16,4},{20,0},{24,12},{28,8},{1,21},{... | collective-permute-start | bytes 49160 | tf_op jit(solution)/shard_map/ppermute | solution.py:34
  60.4 1.1 %collective-permute-done.19 = bf16[16,512]{1,0:T(8,128)(2,1)S(1)} collective-permute-done((bf16[16,512]{1,0:T(8,128)(2,1)S(1)}, bf16[16,512]{1,0:T(8,128)(2,1)S(1)}, u32[]{:S(2)}, u32[]{:S(2)}) %collective-permute-start.19) | collective-permute-done | bytes 16416 | tf_op jit(solution)/shard_map/ppermute | solution.py:34
  61.5 1.9 %collective-permute-done.21 = bf16[16,512]{1,0:T(8,128)(2,1)S(1)} collective-permute-done((bf16[16,512]{1,0:T(8,128)(2,1)S(1)}, bf16[16,512]{1,0:T(8,128)(2,1)S(1)}, u32[]{:S(2)}, u32[]{:S(2)}) %collective-permute-start.21) | collective-permute-done | bytes 16416 | tf_op jit(solution)/shard_map/ppermute | solution.py:34
  63.5 0.6 fusion.3
  (25 shorter events, 2.5 us)
Async XLA Ops:
  0.0 47.9 %collective-permute-start.13 = (bf16[1,2048,512]{2,1,0:T(8,128)(2,1)}, bf16[1,2048,512]{2,1,0:T(8,128)(2,1)S(1)}, u32[]{:S(2)}, u32[]{:S(2)}) collective-permute-start(bf16[1,2048,512]{2,1,0:T(8,128)(2,1)} %refs_0_.5), channel_id=1, source_target_pairs={{0,4},{4,0},{8,12},{12,8},{16,20},{20,16},{24,28},{28,24},{1,5},{5... | collective-permute-start | bytes 6291464 | tf_op jit(solution)/shard_map/ppermute | solution.py:27
  0.5 47.4 %collective-permute-start.14 = (bf16[1,2048,512]{2,1,0:T(8,128)(2,1)}, bf16[1,2048,512]{2,1,0:T(8,128)(2,1)S(1)}, u32[]{:S(2)}, u32[]{:S(2)}) collective-permute-start(bf16[1,2048,512]{2,1,0:T(8,128)(2,1)} %refs_1_.5), channel_id=1, source_target_pairs={{0,4},{4,0},{8,12},{12,8},{16,20},{20,16},{24,28},{28,24},{1,5},{5... | collective-permute-start | bytes 6291464 | tf_op jit(solution)/shard_map/ppermute | solution.py:27
  0.5 47.4 %collective-permute-start.15 = (bf16[1,512,2048]{2,1,0:T(8,128)(2,1)}, bf16[1,512,2048]{2,1,0:T(8,128)(2,1)S(1)}, u32[]{:S(2)}, u32[]{:S(2)}) collective-permute-start(bf16[1,512,2048]{2,1,0:T(8,128)(2,1)} %refs_2_.3), channel_id=1, source_target_pairs={{0,4},{4,0},{8,12},{12,8},{16,20},{20,16},{24,28},{28,24},{1,5},{5... | collective-permute-start | bytes 6291464 | tf_op jit(solution)/shard_map/ppermute | solution.py:27
  2.1 14.9 %collective-permute-start.3 = (bf16[256,896]{1,0:T(8,128)(2,1)S(1)}, bf16[256,896]{1,0:T(8,128)(2,1)S(1)}, u32[]{:S(2)}, u32[]{:S(2)}) collective-permute-start(bf16[256,896]{1,0:T(8,128)(2,1)S(1)} %shard_map.174.refs_4_), channel_id=1, source_target_pairs={{0,4},{4,0},{8,12},{12,8},{16,20},{20,16},{24,28},{28,24},{1,5},{5... | collective-permute-start | bytes 1376264 | tf_op jit(solution)/shard_map/ppermute | solution.py:27
  3.2 4.2 %collective-permute-start = (bf16[16,512]{1,0:T(8,128)(2,1)S(1)}, bf16[16,512]{1,0:T(8,128)(2,1)S(1)}, u32[]{:S(2)}, u32[]{:S(2)}) collective-permute-start(bf16[16,512]{1,0:T(8,128)(2,1)S(1)} %get-tuple-element.36), channel_id=1, source_target_pairs={{0,12},{4,8},{8,4},{12,0},{16,28},{20,24},{24,20},{28,16},{1,13},{... | collective-permute-start | bytes 49160 | tf_op jit(solution)/shard_map/ppermute | solution.py:34
  7.4 4.3 %collective-permute-start.1 = (bf16[16,512]{1,0:T(8,128)(2,1)S(1)}, bf16[16,512]{1,0:T(8,128)(2,1)S(1)}, u32[]{:S(2)}, u32[]{:S(2)}) collective-permute-start(bf16[16,512]{1,0:T(8,128)(2,1)S(1)} %get-tuple-element.37), channel_id=1, source_target_pairs={{0,20},{4,16},{8,28},{12,24},{16,4},{20,0},{24,12},{28,8},{1,21},{... | collective-permute-start | bytes 49160 | tf_op jit(solution)/shard_map/ppermute | solution.py:34
  11.6 5.4 %collective-permute-start.2 = (bf16[16,512]{1,0:T(8,128)(2,1)S(1)}, bf16[16,512]{1,0:T(8,128)(2,1)S(1)}, u32[]{:S(2)}, u32[]{:S(2)}) collective-permute-start(bf16[16,512]{1,0:T(8,128)(2,1)S(1)} %get-tuple-element.38), channel_id=1, source_target_pairs={{0,28},{4,24},{8,20},{12,16},{16,12},{20,8},{24,4},{28,0},{1,29},{... | collective-permute-start | bytes 49160 | tf_op jit(solution)/shard_map/ppermute | solution.py:34
  17.3 4.1 %collective-permute-start.4 = (bf16[16,896]{1,0:T(8,128)(2,1)S(1)}, bf16[16,896]{1,0:T(8,128)(2,1)S(1)}, u32[]{:S(2)}, u32[]{:S(2)}) collective-permute-start(bf16[16,896]{1,0:T(8,128)(2,1)S(1)} %get-tuple-element.40), channel_id=1, source_target_pairs={{0,12},{4,8},{8,4},{12,0},{16,28},{20,24},{24,20},{28,16},{1,13},{... | collective-permute-start | bytes 86024 | tf_op jit(solution)/shard_map/ppermute | solution.py:34
  17.4 8.7 %collective-permute-start.5 = (bf16[16,896]{1,0:T(8,128)(2,1)S(1)}, bf16[16,896]{1,0:T(8,128)(2,1)S(1)}, u32[]{:S(2)}, u32[]{:S(2)}) collective-permute-start(bf16[16,896]{1,0:T(8,128)(2,1)S(1)} %get-tuple-element.41), channel_id=1, source_target_pairs={{0,20},{4,16},{8,28},{12,24},{16,4},{20,0},{24,12},{28,8},{1,21},{... | collective-permute-start | bytes 86024 | tf_op jit(solution)/shard_map/ppermute | solution.py:34
  21.4 5.1 %collective-permute-start.6 = (bf16[16,896]{1,0:T(8,128)(2,1)S(1)}, bf16[16,896]{1,0:T(8,128)(2,1)S(1)}, u32[]{:S(2)}, u32[]{:S(2)}) collective-permute-start(bf16[16,896]{1,0:T(8,128)(2,1)S(1)} %get-tuple-element.42), channel_id=1, source_target_pairs={{0,28},{4,24},{8,20},{12,16},{16,12},{20,8},{24,4},{28,0},{1,29},{... | collective-permute-start | bytes 86024 | tf_op jit(solution)/shard_map/ppermute | solution.py:34
  27.5 5.2 %collective-permute-start.9 = (bf16[16,2048]{1,0:T(8,128)(2,1)S(1)}, bf16[16,2048]{1,0:T(8,128)(2,1)S(1)}, u32[]{:S(2)}, u32[]{:S(2)}) collective-permute-start(bf16[16,2048]{1,0:T(8,128)(2,1)S(1)} %recurrent.1.part_ref), channel_id=1, source_target_pairs={{0,3},{1,2},{2,1},{3,0},{4,7},{5,6},{6,5},{7,4},{8,11},{9,10},{10,... | collective-permute-start | bytes 196616 | tf_op jit(solution)/shard_map/ppermute | solution.py:47
  30.0 4.3 %collective-permute-start.8 = (bf16[16,2048]{1,0:T(8,128)(2,1)S(1)}, bf16[16,2048]{1,0:T(8,128)(2,1)S(1)}, u32[]{:S(2)}, u32[]{:S(2)}) collective-permute-start(bf16[16,2048]{1,0:T(8,128)(2,1)S(1)} %recurrent.1.part_ref), channel_id=1, source_target_pairs={{0,2},{1,3},{2,0},{3,1},{4,6},{5,7},{6,4},{7,5},{8,10},{9,11},{10,... | collective-permute-start | bytes 196616 | tf_op jit(solution)/shard_map/ppermute | solution.py:47
  32.7 4.3 %collective-permute-start.7 = (bf16[16,2048]{1,0:T(8,128)(2,1)S(1)}, bf16[16,2048]{1,0:T(8,128)(2,1)S(1)}, u32[]{:S(2)}, u32[]{:S(2)}) collective-permute-start(bf16[16,2048]{1,0:T(8,128)(2,1)S(1)} %recurrent.1.part_ref), channel_id=1, source_target_pairs={{0,1},{1,0},{2,3},{3,2},{4,5},{5,4},{6,7},{7,6},{8,9},{9,8},{10,11... | collective-permute-start | bytes 196616 | tf_op jit(solution)/shard_map/ppermute | solution.py:47
  37.2 6.4 %collective-permute-start.12 = (bf16[16,2176]{1,0:T(8,128)(2,1)S(1)}, bf16[16,2176]{1,0:T(8,128)(2,1)S(1)}, u32[]{:S(2)}, u32[]{:S(2)}) collective-permute-start(bf16[16,2176]{1,0:T(8,128)(2,1)S(1)} %get-tuple-element.51.refs_0_), channel_id=1, source_target_pairs={{0,28},{4,24},{8,20},{12,16},{16,12},{20,8},{24,4},{28,0},{1,29},{... | collective-permute-start | bytes 208904 | tf_op jit(solution)/shard_map/ppermute | solution.py:34
  37.7 8.9 %collective-permute-start.11 = (bf16[16,2176]{1,0:T(8,128)(2,1)S(1)}, bf16[16,2176]{1,0:T(8,128)(2,1)S(1)}, u32[]{:S(2)}, u32[]{:S(2)}) collective-permute-start(bf16[16,2176]{1,0:T(8,128)(2,1)S(1)} %get-tuple-element.51.refs_0_), channel_id=1, source_target_pairs={{0,20},{4,16},{8,28},{12,24},{16,4},{20,0},{24,12},{28,8},{1,21},{... | collective-permute-start | bytes 208904 | tf_op jit(solution)/shard_map/ppermute | solution.py:34
  43.6 4.3 %collective-permute-start.10 = (bf16[16,2176]{1,0:T(8,128)(2,1)S(1)}, bf16[16,2176]{1,0:T(8,128)(2,1)S(1)}, u32[]{:S(2)}, u32[]{:S(2)}) collective-permute-start(bf16[16,2176]{1,0:T(8,128)(2,1)S(1)} %get-tuple-element.51.refs_0_), channel_id=1, source_target_pairs={{0,12},{4,8},{8,4},{12,0},{16,28},{20,24},{24,20},{28,16},{1,13},{... | collective-permute-start | bytes 208904 | tf_op jit(solution)/shard_map/ppermute | solution.py:34
  50.0 4.3 %collective-permute-start.16 = (bf16[64,512]{1,0:T(8,128)(2,1)S(1)}, bf16[64,512]{1,0:T(8,128)(2,1)S(1)}, u32[]{:S(2)}, u32[]{:S(2)}) collective-permute-start(bf16[64,512]{1,0:T(8,128)(2,1)S(1)} %get-tuple-element.58), channel_id=1, source_target_pairs={{0,1},{1,0},{2,3},{3,2},{4,5},{5,4},{6,7},{7,6},{8,9},{9,8},{10,11... | collective-permute-start | bytes 196616 | tf_op jit(solution)/shard_map/ppermute | solution.py:47
  51.6 4.3 %collective-permute-start.17 = (bf16[64,512]{1,0:T(8,128)(2,1)S(1)}, bf16[64,512]{1,0:T(8,128)(2,1)S(1)}, u32[]{:S(2)}, u32[]{:S(2)}) collective-permute-start(bf16[64,512]{1,0:T(8,128)(2,1)S(1)} %get-tuple-element.59), channel_id=1, source_target_pairs={{0,2},{1,3},{2,0},{3,1},{4,6},{5,7},{6,4},{7,5},{8,10},{9,11},{10,... | collective-permute-start | bytes 196616 | tf_op jit(solution)/shard_map/ppermute | solution.py:47
  53.1 5.2 %collective-permute-start.18 = (bf16[64,512]{1,0:T(8,128)(2,1)S(1)}, bf16[64,512]{1,0:T(8,128)(2,1)S(1)}, u32[]{:S(2)}, u32[]{:S(2)}) collective-permute-start(bf16[64,512]{1,0:T(8,128)(2,1)S(1)} %get-tuple-element.60), channel_id=1, source_target_pairs={{0,3},{1,2},{2,1},{3,0},{4,7},{5,6},{6,5},{7,4},{8,11},{9,10},{10,... | collective-permute-start | bytes 196616 | tf_op jit(solution)/shard_map/ppermute | solution.py:47
  58.3 3.2 %collective-permute-start.19 = (bf16[16,512]{1,0:T(8,128)(2,1)S(1)}, bf16[16,512]{1,0:T(8,128)(2,1)S(1)}, u32[]{:S(2)}, u32[]{:S(2)}) collective-permute-start(bf16[16,512]{1,0:T(8,128)(2,1)S(1)} %get-tuple-element.63), channel_id=1, source_target_pairs={{0,12},{4,8},{8,4},{12,0},{16,28},{20,24},{24,20},{28,16},{1,13},{... | collective-permute-start | bytes 49160 | tf_op jit(solution)/shard_map/ppermute | solution.py:34
  58.4 5.1 %collective-permute-start.21 = (bf16[16,512]{1,0:T(8,128)(2,1)S(1)}, bf16[16,512]{1,0:T(8,128)(2,1)S(1)}, u32[]{:S(2)}, u32[]{:S(2)}) collective-permute-start(bf16[16,512]{1,0:T(8,128)(2,1)S(1)} %get-tuple-element.64), channel_id=1, source_target_pairs={{0,28},{4,24},{8,20},{12,16},{16,12},{20,8},{24,4},{28,0},{1,29},{... | collective-permute-start | bytes 49160 | tf_op jit(solution)/shard_map/ppermute | solution.py:34
  58.5 5.0 %collective-permute-start.20 = (bf16[16,512]{1,0:T(8,128)(2,1)S(1)}, bf16[16,512]{1,0:T(8,128)(2,1)S(1)}, u32[]{:S(2)}, u32[]{:S(2)}) collective-permute-start(bf16[16,512]{1,0:T(8,128)(2,1)S(1)} %get-tuple-element.65), channel_id=1, source_target_pairs={{0,20},{4,16},{8,28},{12,24},{16,4},{20,0},{24,12},{28,8},{1,21},{... | collective-permute-start | bytes 49160 | tf_op jit(solution)/shard_map/ppermute | solution.py:34
